TPU v7x, 32 devices: a whole 2x2x4 slice. The times are simulated.
32 devices in a mesh: sp: 16 (over z, y, x), tp: 2 (over core).
Axes of the slice: x: 2, y: 2, z: 4, core: 2. Of those that a mesh axis runs over, the one named last changes fastest.
Arguments:
- latent: bfloat16 [4096, 2048], P(('sp', 'tp')), may hold values from -6 to 6
- context: bfloat16 [512, 2048], P('sp'), may hold values from -6 to 6
- condition: float32 [2048], P('tp'), may hold values from -6 to 6
- context_condition: float32 [2048], P('tp'), may hold values from -6 to 6
- modulation_weight: bfloat16 [2048, 6144], P('tp', 'sp'), may hold values from -0.125 to 0.125
- query_first: bfloat16 [2048, 512], P(None, 'tp'), may hold values from -1 to 1
- query_second: bfloat16 [2048, 512], P(None, 'tp'), may hold values from -1 to 1
- key_first: bfloat16 [2048, 512], P(None, 'tp'), may hold values from -1 to 1
- key_second: bfloat16 [2048, 512], P(None, 'tp'), may hold values from -1 to 1
- value_weight: bfloat16 [2048, 1024], P(None, 'tp'), may hold values from -0.125 to 0.125
- lambda_head: float32 [8], P('tp'), may hold values from 0.3 to 0.8
- context_score_boost: float32 [8], P('tp'), may hold values from 1.5 to 3
- head_gain: float32 [128], replicated, may hold values from 0.1 to 1.9
- output_weight: bfloat16 [1024, 2048], P('tp'), may hold values from -0.1875 to 0.1875
Outputs:
- updated: bfloat16 [4096, 2048], P(('sp', 'tp'))
All inputs are finite; a program needn't handle non-finite values.
Results may differ from a plain program's by a relative error of at most 0.0095.
Values may be sent and summed in bfloat16 or wider, within the bound.
No kernel may reach another device: no remote copies, remote signals or barrier semaphores. Data moves between devices by JAX's collectives and lax.ppermute only.
A program may use at most 64 MiB of HBM per device.

v0:
```python
import jax
import jax.numpy as jnp
from jax import lax
from jax.sharding import PartitionSpec as P

HEAD_DIM = 64
VALUE_DIM = 128
GRID_W = 64


EPSILON = 1e-06
THETA = 10000.0
NEGATIVE = -1e30


def norm_rows(rows):
    values = rows.astype(jnp.float32)
    return values * lax.rsqrt(jnp.mean(values * values, axis=-1, keepdims=True) + EPSILON)


def rotate_pairs(values, positions):
    half = values.shape[-1] // 2
    quarter = half // 2
    reciprocal_norm = THETA ** (-jnp.arange(quarter, dtype=jnp.float32) / quarter)

    def turn(part, where):
        angle = where.astype(jnp.float32)[:, None] * reciprocal_norm[None, :]
        cosine_table = jnp.concatenate([jnp.cos(angle)] * 2, -1)[:, None, :]
        sine = jnp.concatenate([jnp.sin(angle)] * 2, -1)[:, None, :]
        flipped = jnp.concatenate([-part[..., quarter:], part[..., :quarter]], -1)
        return part * cosine_table + flipped * sine

    grid_row = positions // GRID_W
    grid_col = positions % GRID_W
    return jnp.concatenate(
        [turn(values[..., :half], grid_row), turn(values[..., half:], grid_col)], -1
    )


def block_extent(rows):
    size = min(rows, 1024)
    while rows % size:
        size -= 1
    return size


def body(
    latent,
    context,
    condition,
    context_condition,
    modulation_weight,
    query_first,
    query_second,
    key_first,
    key_second,
    value_weight,
    lambda_head,
    context_score_boost,
    head_gain,
    output_weight,
):
    width = latent.shape[1]
    signal = jax.nn.silu(jnp.stack([condition, context_condition])).astype(jnp.bfloat16)
    partial_mod = jnp.dot(signal, modulation_weight, preferred_element_type=jnp.float32)
    reduced = lax.psum(partial_mod, "tp")
    modulation = lax.all_gather(reduced, "sp", axis=1, tiled=True)
    shift = modulation[:, :width]
    scale = modulation[:, width : 2 * width]
    gate = modulation[:, 2 * width :]
    h_latent = (norm_rows(latent) * (1.0 + scale[0]) + shift[0]).astype(jnp.bfloat16)
    h_context = (norm_rows(context) * (1.0 + scale[1]) + shift[1]).astype(jnp.bfloat16)
    heads_dev = value_weight.shape[1] // VALUE_DIM
    span = heads_dev * HEAD_DIM
    offset = lax.axis_index("sp") * (latent.shape[0] * lax.axis_size("tp"))
    piece = lax.all_gather(h_latent, "tp", axis=0, tiled=True)
    count = piece.shape[0]
    positions = offset + jnp.arange(count, dtype=jnp.int32)
    turned = []
    for weight in (query_first, query_second, key_first, key_second):
        product = jnp.dot(piece, weight, preferred_element_type=jnp.float32).reshape(
            count, heads_dev, HEAD_DIM
        )
        turned.append(rotate_pairs(product, positions).astype(jnp.bfloat16).reshape(count, span))
    values = jnp.dot(piece, value_weight, preferred_element_type=jnp.float32).astype(jnp.bfloat16)
    projected = jnp.concatenate(turned + [values], axis=1)
    queries = projected.shape[0]
    queries_one = projected[:, :span].reshape(queries, heads_dev, HEAD_DIM)
    queries_two = projected[:, span : 2 * span].reshape(queries, heads_dev, HEAD_DIM)
    latent_keys = projected[:, 2 * span : 4 * span]
    latent_values = projected[:, 4 * span :]

    def update(carry, block):
        keys_pair, values, boolean_markers = block
        count = keys_pair.shape[0]
        keys_one = keys_pair[:, :span].reshape(count, heads_dev, HEAD_DIM)
        keys_two = keys_pair[:, span:].reshape(count, heads_dev, HEAD_DIM)
        values_heads = values.reshape(count, heads_dev, VALUE_DIM)
        extra_score = context_score_boost[:, None, None] * boolean_markers[None, None, :]
        renewed = []
        for (highest, totals, weighted), query, keys in zip(
            carry, (queries_one, queries_two), (keys_one, keys_two)
        ):
            scores = (
                jnp.einsum("qhd,khd->hqk", query, keys, preferred_element_type=jnp.float32)
                * HEAD_DIM ** (-0.5)
                + extra_score
            )
            peak = jnp.maximum(highest, jnp.max(scores, axis=-1))
            exp_weights = jnp.exp(scores - peak[..., None])
            rescale = jnp.exp(highest - peak)
            totals = totals * rescale + jnp.sum(exp_weights, axis=-1)
            weighted = weighted * jnp.transpose(rescale)[:, :, None] + jnp.einsum(
                "hqk,khe->qhe",
                exp_weights.astype(jnp.bfloat16),
                values_heads,
                preferred_element_type=jnp.float32,
            )
            renewed.append((peak, totals, weighted))
        return (tuple(renewed), None)

    def fold_keys(carry, keys_pair, values, boolean_markers):
        rows = keys_pair.shape[0]
        size = block_extent(rows)
        count = rows // size
        blocks = (
            keys_pair.reshape(count, size, keys_pair.shape[1]),
            values.reshape(count, size, values.shape[1]),
            boolean_markers.reshape(count, size),
        )
        carry, unused = lax.scan(update, carry, blocks)
        return carry

    start_state = (
        jnp.full((heads_dev, queries), NEGATIVE, jnp.float32),
        jnp.zeros((heads_dev, queries), jnp.float32),
        jnp.zeros((queries, heads_dev, VALUE_DIM), jnp.float32),
    )
    initial = (start_state, start_state)
    keys_pair = jnp.concatenate(
        [
            jnp.dot(h_context, key_first, preferred_element_type=jnp.float32).astype(jnp.bfloat16),
            jnp.dot(h_context, key_second, preferred_element_type=jnp.float32).astype(jnp.bfloat16),
        ],
        axis=1,
    )
    values = jnp.dot(h_context, value_weight, preferred_element_type=jnp.float32).astype(
        jnp.bfloat16
    )
    all_keys, all_values = (
        lax.all_gather(keys_pair, "sp", axis=0, tiled=True),
        lax.all_gather(values, "sp", axis=0, tiled=True),
    )
    carry = fold_keys(initial, all_keys, all_values, jnp.ones((all_keys.shape[0],), jnp.float32))
    pieces = (
        lax.all_gather(latent_keys, "sp", axis=0, tiled=True),
        lax.all_gather(latent_values, "sp", axis=0, tiled=True),
    )
    boolean_markers = jnp.zeros((pieces[0].shape[0],), jnp.float32)
    final = fold_keys(carry, pieces[0], pieces[1], boolean_markers)
    outcomes = [weighted / jnp.transpose(totals)[:, :, None] for highest, totals, weighted in final]
    mixed = outcomes[0] - lambda_head[None, :, None] * outcomes[1]
    normed = (
        mixed * lax.rsqrt(jnp.mean(mixed * mixed, axis=-1, keepdims=True) + EPSILON) * head_gain
    )
    heads_out = normed.astype(jnp.bfloat16).reshape(queries, heads_dev * VALUE_DIM)
    branch = lax.psum_scatter(
        jnp.dot(heads_out, output_weight, preferred_element_type=jnp.float32).astype(jnp.bfloat16),
        "tp",
        scatter_dimension=0,
        tiled=True,
    ).astype(jnp.float32)
    return (latent.astype(jnp.float32) + gate[0] * branch).astype(jnp.bfloat16)


def solution(mesh):
    in_specs = (
        P(("sp", "tp"), None),
        P("sp", None),
        P("tp"),
        P("tp"),
        P("tp", "sp"),
        P(None, "tp"),
        P(None, "tp"),
        P(None, "tp"),
        P(None, "tp"),
        P(None, "tp"),
        P("tp"),
        P("tp"),
        P(),
        P("tp", None),
    )
    out_specs = P(("sp", "tp"), None)
    return jax.shard_map(body, mesh=mesh, in_specs=in_specs, out_specs=out_specs, check_vma=False)
```

profile of v0, /device:TPU:0, one launch (start us, length us, event | category | flops | bytes accessed | tf_op | source)
XLA Modules:
  0.0 315.9 jit_solution(17593726352576110666)
XLA Ops:
  6.5 1.4 fusion.40
  7.9 1.3 fusion.74
  9.3 2.6 psum.7
  11.9 42.5 %all_gather.18 = f32[2,6144]{1,0:T(2,128)S(1)} all-gather(f32[2,384]{1,0:T(2,128)S(1)} %psum.7), channel_id=1, replica_groups=mesh['sp'=16,'tp'=2] {'sp'}, dimensions={1}, use_global_device_ids=true | all-gather | bytes 52224 | tf_op jit(solution)/shard_map/all_gather | solution.py:67
  55.0 2.1 fusion.43
  57.2 5.0 %all-gather.4.cloned.1.call-done = bf16[256,2048]{1,0:T(8,128)(2,1)} async-done(((bf16[128,2048]{1,0:T(8,128)(2,1)}), bf16[256,2048]{1,0:T(8,128)(2,1)}) %all-gather.4.cloned.1.call-update) | async-done | bytes 1048592 | tf_op jit(solution)/shard_map/all_gather | solution.py:76
  62.2 3.4 %convolution_convert_fusion.1 = bf16[256,512]{1,0:T(8,128)(2,1)} fusion(bf16[256,2048]{1,0:T(8,128)(2,1)} %all-gather.4.cloned.1.call-done, bf16[2048,512]{1,0:T(8,128)(2,1)} %param.25), kind=kOutput, calls=%fused_computation.53 | convolution fusion | flops 537001984 | bytes 3407872 | tf_op jit(solution)/shard_map/dot_general | solution.py:85
  66.0 1.8 fusion.99
  68.7 1.8 fusion.100
  73.2 2.1 convolution_convert_fusion.2
  75.3 45.0 %all_gather.21 = bf16[512,512]{1,0:T(8,128)(2,1)S(1)} all-gather(bf16[32,512]{1,0:T(8,128)(2,1)S(1)} %convolution_convert_fusion.2), channel_id=1, replica_groups=mesh['sp'=16,'tp'=2] {'sp'}, dimensions={0}, use_global_device_ids=true | all-gather | bytes 557056 | tf_op jit(solution)/shard_map/all_gather | solution.py:152
  120.5 1.6 convolution_convert_fusion.3
  122.1 1.6 convolution_convert_fusion.4
  123.7 42.0 %all_gather.20 = bf16[512,512]{1,0:T(8,128)(2,1)S(1)} all-gather(bf16[32,512]{1,0:T(8,128)(2,1)S(1)} %pad_maximum_fusion.9), channel_id=1, replica_groups=mesh['sp'=16,'tp'=2] {'sp'}, dimensions={0}, use_global_device_ids=true | all-gather | bytes 557056 | tf_op jit(solution)/shard_map/all_gather | solution.py:151
  166.9 1.4 fusion.89
  170.2 1.5 fusion.38
  171.7 1.5 fusion.39
  173.2 56.5 %all-gather.6.cloned.1.call-done = bf16[4096,512]{1,0:T(8,128)(2,1)} async-done(((bf16[256,512]{1,0:T(8,128)(2,1)}), bf16[4096,512]{1,0:T(8,128)(2,1)}) %all-gather.6.cloned.1.call-update) | async-done | bytes 4194320 | tf_op jit(solution)/shard_map/all_gather | solution.py:156
  229.7 67.3 %while.2 = (s32[]{:T(128)}, f32[4,256]{1,0:T(4,128)S(1)}, f32[4,256]{1,0:T(4,128)S(1)}, f32[256,4,128]{0,2,1:T(8,128)}, f32[4,256]{1,0:T(4,128)S(1)}, /*index=5*...) while((s32[]{:T(128)}, f32[4,256]{1,0:T(4,128)S(1)}, ...), condition=%wide.region_12.13_spmd, body=%wide.region_7.12_spmd.sunk | while | flops 828905472 | bytes 53870940 | solution.py:131
  229.7 2.4 constant_dynamic-slice_fusion.5
  232.1 1.5 copy.40
  233.6 2.4 constant_dynamic-slice_fusion.4
  235.9 2.3 copy.39
  238.2 1.3 fusion.150
  240.3 1.4 bitcast_reduce_fusion.3
  241.7 1.7 fusion.154
  246.5 2.4 constant_dynamic-slice_fusion.5
  248.9 1.5 copy.40
  250.4 2.4 constant_dynamic-slice_fusion.4
  252.7 2.3 copy.39
  257.1 1.4 bitcast_reduce_fusion.3
  258.5 1.7 fusion.154
  263.4 2.4 constant_dynamic-slice_fusion.5
  265.7 1.5 copy.40
  267.2 2.4 constant_dynamic-slice_fusion.4
  269.6 2.3 copy.39
  273.9 1.4 bitcast_reduce_fusion.3
  275.3 1.7 fusion.154
  280.2 2.4 constant_dynamic-slice_fusion.5
  282.5 1.5 copy.40
  284.0 2.4 constant_dynamic-slice_fusion.4
  286.4 2.3 copy.39
  290.7 1.4 bitcast_reduce_fusion.3
  292.1 1.7 fusion.154
  297.0 1.4 multiply_reduce_fusion
  298.5 1.7 convolution_convert_fusion
  300.2 7.2 %reduce-scatter.2.cloned.1.call-done = bf16[128,2048]{1,0:T(8,128)(2,1)} async-done(((bf16[256,2048]{1,0:T(8,128)(2,1)}), bf16[128,2048]{1,0:T(8,128)(2,1)}) %reduce-scatter.2.cloned.1.call-update) | async-done | bytes 524304 | tf_op jit(solution)/shard_map/reduce_scatter | solution.py:167
  307.4 2.0 fusion.44
  (153 shorter events, 27.1 us)
Async XLA Ops:
  6.5 291.9 %copy-start = (bf16[512,2048]{1,0:T(8,128)(2,1)S(1)}, bf16[512,2048]{1,0:T(8,128)(2,1)}, u32[]{:S(2)}) copy-start(bf16[512,2048]{1,0:T(8,128)(2,1)} %param.29) | copy-start | bytes 6291460
  6.5 55.6 %all-gather.4.cloned.1.call-start = ((), (), s32[]{:S(2)}) async-start(), calls=%async_computation.1 | async-start | bytes 1572864 | tf_op jit(solution)/shard_map/all_gather | solution.py:76
  57.1 116.1 %all-gather.8.cloned.1.call-start = ((), (), s32[]{:S(2)}) async-start(), calls=%async_computation.3 | async-start | bytes 4456448 | tf_op jit(solution)/shard_map/all_gather | solution.py:157
  62.2 3.8 %copy-start.5 = (bf16[256,2048]{1,0:T(8,128)(2,1)S(1)}, bf16[256,2048]{1,0:T(8,128)(2,1)}, u32[]{:S(2)}) copy-start(bf16[256,2048]{1,0:T(8,128)(2,1)} %all-gather.4.cloned.1.call-done) | copy-start | bytes 3145732
  65.6 164.1 %all-gather.6.cloned.1.call-start = ((), (), s32[]{:S(2)}) async-start(), calls=%async_computation.2 | async-start | bytes 4456448 | tf_op jit(solution)/shard_map/all_gather | solution.py:156
  65.6 2.1 copy-start.8
  65.9 2.5 copy-start.10
  65.9 2.5 copy-start.12
  66.0 2.5 copy-start.14
  66.0 2.4 copy-start.16
  68.7 1.9 copy-start.9
  70.5 0.8 copy-start.11
  70.5 0.8 copy-start.13
  70.6 0.8 copy-start.15
  70.6 0.8 copy-start.17
  71.1 1.9 copy-start.7
  73.0 234.4 %reduce-scatter.2.cloned.1.call-start = ((), (), s32[]{:S(2)}) async-start(), calls=%async_computation.4 | async-start | bytes 1572864 | tf_op jit(solution)/shard_map/reduce_scatter | solution.py:167
  165.7 2.6 copy-start.19
  229.7 67.3 %copy-start.20 = (f32[4]{0:T(128)S(1)}, f32[4]{0:T(128)}, u32[]{:S(2)}) copy-start(f32[4]{0:T(128)} %param.26) | copy-start | bytes 52
  229.7 68.7 %copy-start.21 = (f32[128]{0:T(128)S(1)}, f32[128]{0:T(128)}, u32[]{:S(2)}) copy-start(f32[128]{0:T(128)} %param.28) | copy-start | bytes 1540
  241.7 1.7 copy-start.3
  243.4 1.2 copy-start.1
  244.6 1.2 copy-start.4
  245.7 0.8 copy-start.2
  258.5 1.7 copy-start.3
  260.2 1.2 copy-start.1
  261.4 1.2 copy-start.4
  262.5 0.8 copy-start.2
  275.3 1.7 copy-start.3
  277.0 1.2 copy-start.1
  278.2 1.2 copy-start.4
  279.4 0.8 copy-start.2
  292.1 1.7 copy-start.3
  293.8 1.2 copy-start.1
  295.0 1.2 copy-start.4
  296.2 0.8 copy-start.2
  298.5 8.9 %copy-start.6 = (bf16[128,2048]{1,0:T(8,128)(2,1)S(1)}, bf16[128,2048]{1,0:T(8,128)(2,1)}, u32[]{:S(2)}) copy-start(bf16[128,2048]{1,0:T(8,128)(2,1)} %param.16) | copy-start | bytes 1572868
  298.5 8.9 %copy-start.18 = (f32[1,2048]{1,0:T(1,128)S(1)}, f32[1,2048]{1,0:T(1,128)}, u32[]{:S(2)}) copy-start(f32[1,2048]{1,0:T(1,128)} %get-tuple-element.207) | copy-start | bytes 24580
Sparse Core Ops, SparseCore 0:
  57.2 4.8 all-gather.3
  65.7 86.1 all-gather.7
  154.7 74.9 all-gather.5
  300.4 6.9 reduce-scatter.1
where the time goes:
time: 317 us; the launch traced here: 316 us
  blocking collectives  132 us (42%)
  waiting for transfers between devices  68.7 us (22%)
  local copies, waits for them, and re-layouts  43 us (14%)
  matrix products  39.2 us (12%)
  other arithmetic  18.8 us (6%)
  between operations  13.6 us (4%)
    all_gather x1, waiting for transfers between devices, body(): lax.all_gather(latent_keys, 'sp', axis=0, tiled=True)  56.5 us
    all_gather x1, blocking collectives, body(): lax.all_gather(values, 'sp', axis=0, tiled=True)  45 us
    all_gather x1, blocking collectives, body(): modulation = lax.all_gather(reduced, 'sp', axis=1, tiled=True)  42.5 us
    all_gather x1, blocking collectives, body(): lax.all_gather(keys_pair, 'sp', axis=0, tiled=True)  42 us
    dynamic_slice x16, local copies, waits for them, and re-layouts, fold_keys(): carry, unused = lax.scan(update, carry, blocks)  33.9 us
    dot_general x10, matrix products, update(): jnp.einsum('hqk,khe->qhe', exp_weights.astype(jnp.bfloat16), values_heads...  12.1 us
    dot_general x10, matrix products, update(): jnp.einsum('qhd,khd->hqk', query, keys, preferred_element_type=jnp.float32)  10.6 us
    reduce_sum x5, other arithmetic, update(): totals = totals * rescale + jnp.sum(exp_weights, axis=-1)  8.09 us
  transfers between devices with their start and end apart: 4, of which 3 were waited for; matrix products, arithmetic and copies ran while one was open for 6% of the time, Pallas kernels for 0%

commit v1 on v0

v1 whole, which is shorter than its diff:
```python
import functools
import math

import jax
import jax.numpy as jnp
from jax import lax
from jax.experimental import pallas as pl
from jax.experimental.pallas import tpu as pltpu
from jax.sharding import Mesh, PartitionSpec as P

HEAD_DIM = 64
VALUE_DIM = 128
GRID_W = 64
EPSILON = 1e-06
THETA = 10000.0
SP = ("g", "s")
ALL = ("g", "s", "tp")


def norm_rows(rows):
    values = rows.astype(jnp.float32)
    return values * lax.rsqrt(jnp.mean(values * values, axis=-1, keepdims=True) + EPSILON)


def shifts_over(array, axis, size):
    out = [array]
    for k in range(1, size):
        out.append(lax.ppermute(array, axis, [(i, (i + k) % size) for i in range(size)]))
    return out


def in_order(parts, index):
    size = len(parts)
    if size == 1:
        return jnp.stack(parts)
    if size == 2:
        a, b = parts
        first = index == 0
        return jnp.stack([jnp.where(first, a, b), jnp.where(first, b, a)])
    stacked = jnp.stack(parts)
    return jnp.take(stacked, (index - jnp.arange(size)) % size, axis=0)


def rope_tables(positions, extra):
    quarter = HEAD_DIM // 4
    reciprocal = THETA ** (-jnp.arange(quarter, dtype=jnp.float32) / quarter)
    row = (positions // GRID_W).astype(jnp.float32)[:, None] * reciprocal[None, :]
    col = (positions % GRID_W).astype(jnp.float32)[:, None] * reciprocal[None, :]
    angle = jnp.concatenate([row, row, col, col] * 2, -1)
    sign = jnp.where((jnp.arange(2 * HEAD_DIM) // quarter) % 2 == 0, -1.0, 1.0)
    cosine = jnp.cos(angle)
    sine = jnp.sin(angle) * sign[None, :]
    width = angle.shape[1]
    cosine = jnp.concatenate([cosine, jnp.ones((extra, width), jnp.float32)], 0)
    sine = jnp.concatenate([sine, jnp.zeros((extra, width), jnp.float32)], 0)
    return cosine, sine


def attention_kernel(first, last, scal, gain, q_ref, kv_ref, ctx_ref, *refs):
    refs = list(refs)
    vaug, vctx = refs[-2:]
    refs = refs[:-2]
    if not first:
        old, refs = refs[:4], refs[4:]
    out = refs

    @pl.when(pl.program_id(0) == 0)
    def _():
        vaug[:, :VALUE_DIM] = kv_ref[:, 2 * HEAD_DIM :]
        vaug[:, VALUE_DIM:] = jnp.ones((vaug.shape[0], VALUE_DIM), vaug.dtype)
        vctx[:, :VALUE_DIM] = ctx_ref[:, 2 * HEAD_DIM :]
        vctx[:, VALUE_DIM:] = jnp.ones((vctx.shape[0], VALUE_DIM), vctx.dtype)

    q = q_ref[...]
    lane = lax.broadcasted_iota(jnp.int32, q.shape, 1)
    boost = scal[0]
    dims = (((1,), (1,)), ((), ()))
    results = []
    for m in range(2):
        query = jnp.where((lane < HEAD_DIM) == (m == 0), q, jnp.zeros_like(q))
        s_lat = lax.dot_general(
            query, kv_ref[:, : 2 * HEAD_DIM], dims, preferred_element_type=jnp.float32
        )
        s_ctx = lax.dot_general(
            query, ctx_ref[:, : 2 * HEAD_DIM], dims, preferred_element_type=jnp.float32
        ) + boost
        peak = jnp.maximum(
            jnp.max(s_lat, axis=-1, keepdims=True), jnp.max(s_ctx, axis=-1, keepdims=True)
        )
        if not first:
            before = old[2 + m][...][:, :1]
            peak = jnp.maximum(peak, before)
        p_lat = jnp.exp2(s_lat - peak).astype(jnp.bfloat16)
        p_ctx = jnp.exp2(s_ctx - peak).astype(jnp.bfloat16)
        acc = jnp.dot(p_lat, vaug[...], preferred_element_type=jnp.float32) + jnp.dot(
            p_ctx, vctx[...], preferred_element_type=jnp.float32
        )
        if not first:
            acc = acc + old[m][...] * jnp.exp2(before - peak)
        if last:
            results.append(acc[:, :VALUE_DIM] / acc[:, VALUE_DIM:])
        else:
            out[m][...] = acc
            out[2 + m][...] = jnp.broadcast_to(peak, (q.shape[0], 128))
    if last:
        mixed = results[0] - scal[1] * results[1]
        scale = lax.rsqrt(jnp.mean(mixed * mixed, axis=-1, keepdims=True) + EPSILON)
        out[0][...] = (mixed * scale * gain[...]).astype(out[0].dtype)


def attend(scal, gain, queries, kv, ctx, state, last):
    count = queries.shape[0]
    tile = math.gcd(count, 256)
    rows = lambda width: pl.BlockSpec((tile, width), lambda i: (i, 0))
    whole = lambda a: pl.BlockSpec(a.shape, lambda i: (0, 0))
    state_shapes = [jax.ShapeDtypeStruct((count, w), jnp.float32) for w in (256, 256, 128, 128)]
    state_specs = [rows(s.shape[1]) for s in state_shapes]
    first = state is None
    if last:
        shapes = jax.ShapeDtypeStruct((count, VALUE_DIM), jnp.bfloat16)
        specs = rows(VALUE_DIM)
    else:
        shapes, specs = state_shapes, state_specs
    return pl.pallas_call(
        functools.partial(attention_kernel, first, last),
        grid=(count // tile,),
        in_specs=[pl.BlockSpec(memory_space=pltpu.SMEM), whole(gain), rows(128), whole(kv), whole(ctx)]
        + ([] if first else state_specs),
        out_specs=specs,
        out_shape=shapes,
        scratch_shapes=[
            pltpu.VMEM((kv.shape[0], 2 * VALUE_DIM), jnp.bfloat16),
            pltpu.VMEM((ctx.shape[0], 2 * VALUE_DIM), jnp.bfloat16),
        ],
        compiler_params=pltpu.CompilerParams(
            dimension_semantics=("arbitrary",), vmem_limit_bytes=56 * 2**20
        ),
        name="attend_last" if last else "attend_first" if first else "attend_next",
    )(scal, gain, queries, kv, ctx, *([] if first else state))


def body(
    latent,
    context,
    condition,
    context_condition,
    modulation_weight,
    query_first,
    query_second,
    key_first,
    key_second,
    value_weight,
    lambda_head,
    context_score_boost,
    head_gain,
    output_weight,
):
    width = latent.shape[1]
    tp = lax.axis_size("tp")
    sp = lax.axis_size(SP)
    groups = lax.axis_size("g")
    t = lax.axis_index("tp")
    head = lax.axis_index("s")
    heads_dev = value_weight.shape[1] // VALUE_DIM
    heads = heads_dev * tp

    signal = jax.nn.silu(jnp.stack([condition, context_condition])).astype(jnp.bfloat16)
    partial_mod = jnp.dot(signal, modulation_weight, preferred_element_type=jnp.float32)
    columns = partial_mod.shape[1]
    message = jnp.concatenate([partial_mod.reshape(-1), lambda_head, context_score_boost])
    pad = -message.shape[0] % 128
    message = jnp.pad(message, (0, pad))
    received = lax.all_to_all(
        jnp.broadcast_to(message[None], (sp * tp, message.shape[0])), ALL, 0, 0
    ).reshape(sp, tp, -1)
    modulation = jnp.sum(received[:, :, : 2 * columns], axis=1).reshape(sp, 2, columns)
    modulation = jnp.transpose(modulation, (1, 0, 2)).reshape(2, sp * columns)
    lambdas = received[0, :, 2 * columns : 2 * columns + heads_dev].reshape(heads)
    boosts = received[0, :, 2 * columns + heads_dev : 2 * columns + 2 * heads_dev].reshape(heads)
    scal = jnp.stack([boosts[head] * math.log2(math.e), lambdas[head]])
    shift = modulation[:, :width]
    scale = modulation[:, width : 2 * width]
    gate = modulation[0, 2 * width :]

    packs = [
        shifts_over(w, "tp", tp)
        for w in (query_first, query_second, key_first, key_second, value_weight)
    ]
    out_weights = shifts_over(output_weight, "tp", tp)
    rows = latent.shape[0]
    rows_ctx = context.shape[0] // tp
    ctx_own = lax.dynamic_slice_in_dim(context, t * rows_ctx, rows_ctx, 0)
    h_latent = (norm_rows(latent) * (1.0 + scale[0]) + shift[0]).astype(jnp.bfloat16)
    h_context = (norm_rows(ctx_own) * (1.0 + scale[1]) + shift[1]).astype(jnp.bfloat16)
    h = jnp.concatenate([h_latent, h_context], 0)
    offset = (lax.axis_index(SP) * tp + t) * rows
    cosine, sine = rope_tables(offset + jnp.arange(rows, dtype=jnp.int32), rows_ctx)
    quarter = HEAD_DIM // 4

    def project(weight, turn, factor=None):
        product = jnp.dot(h, weight, preferred_element_type=jnp.float32)
        if turn:
            reps = product.shape[1] // HEAD_DIM
            table_c = jnp.tile(cosine[:, :HEAD_DIM], (1, reps))
            table_s = jnp.tile(sine[:, :HEAD_DIM], (1, reps))
            lower = (jnp.arange(product.shape[1]) // quarter) % 2 == 0
            flipped = jnp.where(
                lower[None, :], jnp.roll(product, -quarter, 1), jnp.roll(product, quarter, 1)
            )
            product = product * table_c + flipped * table_s
            if factor is not None:
                product = product * factor
        return product.astype(jnp.bfloat16).reshape(h.shape[0], heads_dev, -1)

    factor = HEAD_DIM ** (-0.5) * math.log2(math.e)
    q_parts, kv_parts = [], []
    for k in range(tp):
        q1, q2, k1, k2 = (
            project(packs[n][k], True, factor if n < 2 else None) for n in range(4)
        )
        v = project(packs[4][k], False)
        q_parts.append(jnp.transpose(jnp.concatenate([q1, q2], -1)[:rows], (1, 0, 2)))
        kv_parts.append(jnp.transpose(jnp.concatenate([k1, k2, v], -1), (1, 0, 2)))
    q_all = in_order(q_parts, t).reshape(heads, rows, 2 * HEAD_DIM)
    kv_all = in_order(kv_parts, t).reshape(heads, rows + rows_ctx, 2 * HEAD_DIM + VALUE_DIM)

    queries = lax.all_to_all(q_all, "s", 0, 0).reshape(heads * rows, 2 * HEAD_DIM)
    kv_sent = jnp.broadcast_to(kv_all[None], (groups,) + kv_all.shape)
    kv_sent = kv_sent.reshape((sp,) + kv_all.shape[1:])
    kv = lax.all_to_all(kv_sent, SP, 0, 0)
    kv_each = shifts_over(kv, "tp", tp)
    gain = head_gain[None, :]
    state = None
    for k, part in enumerate(kv_each):
        lat = part[:, :rows].reshape(sp * rows, -1)
        ctx = part[:, rows:].reshape(sp * rows_ctx, -1)
        state = attend(scal, gain, queries, lat, ctx, state, k == tp - 1)
    heads_out = lax.all_to_all(state.reshape(heads, rows, VALUE_DIM), "s", 0, 0)

    grouped = heads_out.reshape(tp, heads_dev, rows, VALUE_DIM)
    branch = 0.0
    for k in range(tp):
        own = lax.dynamic_index_in_dim(grouped, (t - k) % tp, 0, keepdims=False)
        own = jnp.transpose(own, (1, 0, 2)).reshape(rows, heads_dev * VALUE_DIM)
        branch = branch + jnp.dot(own, out_weights[k], preferred_element_type=jnp.float32)
    return (latent.astype(jnp.float32) + gate[None, :] * branch).astype(jnp.bfloat16)


def solution(mesh):
    sp, tp = mesh.shape["sp"], mesh.shape["tp"]

    def run(*args):
        heads = args[9].shape[1] // VALUE_DIM
        inner = Mesh(mesh.devices.reshape(sp // heads, heads, tp), ALL)
        in_specs = (
            P(ALL, None),
            P(SP, None),
            P("tp"),
            P("tp"),
            P("tp", SP),
            P(None, "tp"),
            P(None, "tp"),
            P(None, "tp"),
            P(None, "tp"),
            P(None, "tp"),
            P("tp"),
            P("tp"),
            P(),
            P("tp", None),
        )
        return jax.shard_map(
            body, mesh=inner, in_specs=in_specs, out_specs=P(ALL, None), check_vma=False
        )(*args)

    return run
```

time: 317 us -> 133 us (0.42)
  blocking collectives: 132 us -> 0 us
  waiting for transfers between devices: 68.7 us -> 36 us
  Pallas kernels: 0 us -> 23.3 us
  starting transfers between devices: 0.13 us -> 22.8 us
  local copies, waits for them, and re-layouts: 43 us -> 21.9 us
  matrix products: 39.2 us -> 19.1 us
  between operations: 13.6 us -> 1.37 us
  other arithmetic: 18.8 us -> 7.39 us
    all_gather x3 -> x0, blocking collectives: 129 us -> none  [the longest x1 45 us: body(): lax.all_gather(values, 'sp', axis=0, tiled=True)]
    all_gather x3 -> x0, waiting for transfers between devices: 61.5 us -> none  [the longest x1 56.5 us: body(): lax.all_gather(latent_keys, 'sp', axis=0, tiled=True)]
    all_to_all x0 -> x4, waiting for transfers between devices: none -> 36 us  [the longest x1 22.9 us: body(): kv = lax.all_to_all(kv_sent, SP, 0, 0)]
    dynamic_slice x16 -> x3, local copies, waits for them, and re-layouts: 33.9 us -> 2.93 us  [the longest x1 1.64 us: body(): own = lax.dynamic_index_in_dim(grouped, (t - k) % tp, 0, keepdims=False)]
    pallas_call x0 -> x2, Pallas kernels: none -> 23.3 us  [attend(): pl.pallas_call(functools.partial(attention_kernel, first, last), grid=(co...]
    all_to_all x0 -> x4, starting transfers between devices: none -> 21.2 us  [the longest x1 7.33 us: body(): lax.all_to_all(jnp.broadcast_to(message[None], (sp * tp, message.shape[0]...]
    dot_general x29 -> x12, matrix products: 37.8 us -> 18.2 us  [the longest x10 14 us: project(): product = jnp.dot(h, weight, preferred_element_type=jnp.float32)]
    reduce_sum x6 -> x1, other arithmetic: 9.44 us -> 0.1 us  [body(): jnp.sum(received[:, :, :2 * columns], axis=1).reshape(sp, 2, columns)]
  transfers between devices with their start and end apart: 4 -> 11, of which waited for: 3 -> 4; matrix products, arithmetic and copies ran while one was open for 6% -> 28% of each run, Pallas kernels for 0% -> 18%
where the time goes in v1:
time: 133 us; the launch traced here: 132 us
  waiting for transfers between devices  36 us (27%)
  Pallas kernels  23.3 us (18%)
  starting transfers between devices  22.8 us (17%)
  local copies, waits for them, and re-layouts  21.9 us (16%)
  matrix products  19.1 us (14%)
  other arithmetic  7.39 us (6%)
  between operations  1.37 us (1%)
    pallas_call x2, Pallas kernels, attend(): pl.pallas_call(functools.partial(attention_kernel, first, last), grid=(co...  23.3 us
    all_to_all x1, waiting for transfers between devices, body(): kv = lax.all_to_all(kv_sent, SP, 0, 0)  22.9 us
    dot_general x10, matrix products, project(): product = jnp.dot(h, weight, preferred_element_type=jnp.float32)  14 us
    all_to_all x1, starting transfers between devices, body(): lax.all_to_all(jnp.broadcast_to(message[None], (sp * tp, message.shape[0]...  7.33 us
    all_to_all x1, waiting for transfers between devices, body(): heads_out = lax.all_to_all(state.reshape(heads, rows, VALUE_DIM), 's', 0, 0)  6.6 us
    all_to_all x1, starting transfers between devices, body(): lax.all_to_all(q_all, 's', 0, 0).reshape(heads * rows, 2 * HEAD_DIM)  6.18 us
    all_to_all x1, waiting for transfers between devices, body(): lax.all_to_all(jnp.broadcast_to(message[None], (sp * tp, message.shape[0]...  5.12 us
    dot_general x2, matrix products, body(): jnp.dot(own, out_weights[k], preferred_element_type=jnp.float32)  4.26 us
  transfers between devices with their start and end apart: 11, of which 4 were waited for; matrix products, arithmetic and copies ran while one was open for 28% of the time, Pallas kernels for 18%

profile of v1, /device:TPU:0, one launch (start us, length us, event | category | flops | bytes accessed | tf_op | source)
XLA Modules:
  0.0 131.9 jit_solution(6091666446146947874)
XLA Ops:
  0.0 1.1 copy-done
  1.1 0.9 fusion.42
  2.1 0.8 select_maximum_fusion
  2.9 0.7 broadcast_in_dim.86
  3.6 7.3 %all-to-all-start = ((f32[32,1,896]{2,1,0:T(1,128)}), f32[32,1,896]{2,1,0:T(1,128)S(1)}, u32[]{:S(2)}, u32[]{:S(2)}) async-start(f32[32,1,896]{2,1,0:T(1,128)} %broadcast_in_dim.86), calls=%async_computation | async-start | bytes 229376 | tf_op jit(solution)/shard_map/all_to_all | solution.py:173
  10.9 0.3 collective-permute-start.1
  13.8 5.1 %all-to-all-done = f32[32,1,896]{2,1,0:T(1,128)S(1)} async-done(((f32[32,1,896]{2,1,0:T(1,128)}), f32[32,1,896]{2,1,0:T(1,128)S(1)}, u32[]{:S(2)}, u32[]{:S(2)}) %all-to-all-start) | async-done | bytes 114720 | tf_op jit(solution)/shard_map/all_to_all | solution.py:173
  19.6 0.3 copy-done.5
  20.1 1.8 %fusion.54 = f32[144,256]{1,0:T(8,128)S(1)} fusion(bf16[2048,256]{1,0:T(8,128)(2,1)} %param.22, bf16[16,2048]{1,0:T(8,128)(2,1)S(1)} %fusion.40, bf16[128,2048]{1,0:T(8,128)(2,1)S(1)} %fusion.8), kind=kOutput, calls=%fused_computation.121 | convolution fusion | flops 152174592 | bytes 1785856 | tf_op jit(solution)/shard_map/dot_general | solution.py:201
  22.0 0.3 fusion.55
  22.3 0.5 fusion.3
  23.2 1.5 %fusion.52 = f32[144,256]{1,0:T(8,128)S(1)} fusion(bf16[2048,256]{1,0:T(8,128)(2,1)} %collective-permute-done.3, bf16[16,2048]{1,0:T(8,128)(2,1)S(1)} %fusion.40, bf16[128,2048]{1,0:T(8,128)(2,1)S(1)} %fusion.8), kind=kOutput, calls=%fused_computation.119 | convolution fusion | flops 152174592 | bytes 1785856 | tf_op jit(solution)/shard_map/dot_general | solution.py:201
  24.8 1.6 %fusion.53 = f32[144,256]{1,0:T(8,128)S(1)} fusion(bf16[2048,256]{1,0:T(8,128)(2,1)} %collective-permute-done.2, bf16[16,2048]{1,0:T(8,128)(2,1)S(1)} %fusion.40, bf16[128,2048]{1,0:T(8,128)(2,1)S(1)} %fusion.8), kind=kOutput, calls=%fused_computation.120 | convolution fusion | flops 152174592 | bytes 1785856 | tf_op jit(solution)/shard_map/dot_general | solution.py:201
  27.4 1.6 %fusion.56 = f32[144,256]{1,0:T(8,128)S(1)} fusion(bf16[2048,256]{1,0:T(8,128)(2,1)} %collective-permute-done.1, bf16[16,2048]{1,0:T(8,128)(2,1)S(1)} %fusion.40, bf16[128,2048]{1,0:T(8,128)(2,1)S(1)} %fusion.8), kind=kOutput, calls=%fused_computation.123 | convolution fusion | flops 152174592 | bytes 1785856 | tf_op jit(solution)/shard_map/dot_general | solution.py:201
  29.0 1.6 %fusion.57 = f32[144,256]{1,0:T(8,128)S(1)} fusion(bf16[2048,256]{1,0:T(8,128)(2,1)} %collective-permute-done, bf16[16,2048]{1,0:T(8,128)(2,1)S(1)} %fusion.40, bf16[128,2048]{1,0:T(8,128)(2,1)S(1)} %fusion.8), kind=kOutput, calls=%fused_computation.124 | convolution fusion | flops 152174592 | bytes 1785856 | tf_op jit(solution)/shard_map/dot_general | solution.py:201
  30.9 0.9 fusion.30
  32.1 2.1 %fusion.4 = bf16[18,4,8,128]{3,2,1,0:T(8,128)(2,1)S(1)} fusion(bf16[2048,512]{1,0:T(8,128)(2,1)} %collective-permute-done.4, bf16[16,2048]{1,0:T(8,128)(2,1)} %copy-done.8, bf16[128,2048]{1,0:T(8,128)(2,1)S(1)} %fusion.8), kind=kOutput, calls=%fused_computation.9 | convolution fusion | flops 303243264 | bytes 2834432 | tf_op jit(solution)/shard_map/dot_general | solution.py:201
  34.6 1.1 broadcast_in_dim.92
  35.7 3.7 %all-to-all-start.2 = ((bf16[16,144,256]{2,1,0:T(8,128)(2,1)}), bf16[16,144,256]{2,1,0:T(8,128)(2,1)S(1)}, u32[]{:S(2)}, u32[]{:S(2)}) async-start(bf16[16,144,256]{2,1,0:T(8,128)(2,1)} %bitcast.72), calls=%async_computation.2 | async-start | bytes 2359296 | tf_op jit(solution)/shard_map/all_to_all | solution.py:230
  39.6 1.7 %fusion.59 = f32[144,256]{1,0:T(8,128)S(1)} fusion(bf16[2048,256]{1,0:T(8,128)(2,1)} %param.19, bf16[16,2048]{1,0:T(8,128)(2,1)} %copy-done.8, bf16[128,2048]{1,0:T(8,128)(2,1)S(1)} %fusion.8), kind=kOutput, calls=%fused_computation.126 | convolution fusion | flops 152174592 | bytes 1785856 | tf_op jit(solution)/shard_map/dot_general | solution.py:201
  41.3 0.7 fusion.72
  42.2 1.4 %fusion.58 = f32[144,256]{1,0:T(8,128)S(1)} fusion(bf16[2048,256]{1,0:T(8,128)(2,1)S(1)} %copy-done.12, bf16[16,2048]{1,0:T(8,128)(2,1)S(1)} %copy-done.9, bf16[128,2048]{1,0:T(8,128)(2,1)} %copy-done.4), kind=kOutput, calls=%fused_computation.125 | convolution fusion | flops 152174592 | bytes 1785856 | tf_op jit(solution)/shard_map/dot_general | solution.py:201
  43.6 22.9 %all-to-all-done.2 = bf16[16,144,256]{2,1,0:T(8,128)(2,1)S(1)} async-done(((bf16[16,144,256]{2,1,0:T(8,128)(2,1)}), bf16[16,144,256]{2,1,0:T(8,128)(2,1)S(1)}, u32[]{:S(2)}, u32[]{:S(2)}) %all-to-all-start.2) | async-done | bytes 1179680 | tf_op jit(solution)/shard_map/all_to_all | solution.py:230
  66.7 1.8 %fusion.12 = (bf16[144,256]{1,0:T(8,128)(2,1)}, bf16[144,256]{1,0:T(8,128)(2,1)}) fusion(f32[144,256]{1,0:T(8,128)S(1)} %tile.11, f32[144,16]{1,0:T(8,128)} %get-tuple-element.52, f32[144,240]{1,0:T(8,128)S(1)} %get-tuple-element.54, f32[144,240]{1,0:T(8,128)S(1)} %get-tuple-element.53, f32[144,16]{1,0:T(8,128)} %get-tuple-element.51, ...), kind=kLoop, calls=%fused_computation.29 | loop fusion | flops 589824 | bytes 1327360 | tf_op jit(solution)/shard_map/convert_element_type | solution.py:213
  68.5 1.0 reshape.206
  69.5 1.0 reshape.205
  70.8 0.4 select_bitcast_fusion.3
  71.4 0.7 copy.33
  72.1 6.2 %all-to-all-start.1 = ((bf16[8,128,128]{2,1,0:T(8,128)(2,1)}), bf16[8,128,128]{2,1,0:T(8,128)(2,1)S(1)}, u32[]{:S(2)}, u32[]{:S(2)}) async-start(bf16[8,128,128]{2,1,0:T(8,128)(2,1)} %bitcast.15), calls=%async_computation.1 | async-start | bytes 524288 | tf_op jit(solution)/shard_map/all_to_all | solution.py:227
  78.3 0.8 fusion.76
  79.3 0.6 dynamic_slice.17
  79.9 0.7 dynamic_slice.16
  81.3 1.3 pad_maximum_fusion.8.scal
  82.6 1.1 slice.258
  83.7 0.7 slice.259
  84.3 1.3 all-to-all-done.1
  85.6 0.7 copy-done.2
  86.3 10.9 %attend_first.1 = (f32[1024,256]{1,0:T(8,128)}, f32[1024,256]{1,0:T(8,128)}, f32[1024,128]{1,0:T(8,128)}, f32[1024,128]{1,0:T(8,128)}) custom-call(f32[2]{0:T(128)} %pad_maximum_fusion.8.scal, f32[1,128]{1,0:T(1,128)} %bitcast.93, bf16[1024,128]{1,0:T(8,128)(2,1)} %bitcast.76, bf16[2048,256]{1,0:T(8,128)(2,1)} %bitcast.73, bf16[256,256]{1,0:T(8,128)(2,1)} %bitcast.81), custom_call_target="tpu_custom_call" | custom-call | tf_op jit(solution)/shard_map/attend_first/pallas_call | solution.py:124
  97.3 2.3 %slice.256 = bf16[16,128,256]{2,1,0:T(8,128)(2,1)} slice(bf16[16,144,256]{2,1,0:T(8,128)(2,1)} %collective-permute-done.5), slice={[0:16], [0:128], [0:256]} | slice | bytes 2097152 | tf_op jit(solution)/shard_map/slice | solution.py:235
  99.6 1.6 %slice.257 = bf16[16,16,256]{2,1,0:T(8,128)(2,1)} slice(bf16[16,144,256]{2,1,0:T(8,128)(2,1)} %collective-permute-done.5), slice={[0:16], [128:144], [0:256]} | slice | bytes 262144 | tf_op jit(solution)/shard_map/slice | solution.py:236
  101.1 12.4 %attend_last.1 = bf16[1024,128]{1,0:T(8,128)(2,1)} custom-call(f32[2]{0:T(128)} %pad_maximum_fusion.8.scal, f32[1,128]{1,0:T(1,128)} %bitcast.94, bf16[1024,128]{1,0:T(8,128)(2,1)} %bitcast.77, bf16[2048,256]{1,0:T(8,128)(2,1)} %bitcast.74, bf16[256,256]{1,0:T(8,128)(2,1)} %bitcast.84, f32[1024,256]{1,0:T(8,128)} %get-tuple-element.9.refs_0_, ...), custom_call_target="tpu_custom_call" | custom-call | tf_op jit(solution)/shard_map/attend_last/pallas_call | solution.py:124
  113.5 4.0 %all-to-all-start.3 = ((bf16[8,128,128]{2,1,0:T(8,128)(2,1)}), bf16[8,128,128]{2,1,0:T(8,128)(2,1)}, u32[]{:S(2)}, u32[]{:S(2)}) async-start(bf16[8,128,128]{2,1,0:T(8,128)(2,1)} %bitcast.78), calls=%async_computation.3 | async-start | bytes 524288 | tf_op jit(solution)/shard_map/all_to_all | solution.py:238
  117.6 6.6 %all-to-all-done.3 = bf16[8,128,128]{2,1,0:T(8,128)(2,1)} async-done(((bf16[8,128,128]{2,1,0:T(8,128)(2,1)}), bf16[8,128,128]{2,1,0:T(8,128)(2,1)}, u32[]{:S(2)}, u32[]{:S(2)}) %all-to-all-start.3) | async-done | bytes 262176 | tf_op jit(solution)/shard_map/all_to_all | solution.py:238
  124.2 1.6 %constant_dynamic-slice_fusion = (bf16[1,4,128,128]{3,2,1,0:T(8,128)(2,1)}, bf16[1,4,128,128]{3,2,1,0:T(8,128)(2,1)S(1)}) fusion(bf16[2,4,128,128]{3,2,1,0:T(8,128)(2,1)} %bitcast.28, s32[]{:T(128)S(6)} %select_n.226, s32[]{:T(128)S(6)} %select_n.224), kind=kLoop, calls=%fused_computation.107 | loop fusion | bytes 524296 | tf_op jit(solution)/shard_map/jit(dynamic_index_in_dim)/dynamic_slice | solution.py:243
  125.8 0.8 copy.43
  126.6 1.0 copy.44
  127.6 1.4 %fusion.79 = f32[128,2048]{1,0:T(8,128)S(1)} fusion(bf16[128,512]{0,1:T(8,128)(2,1)} %bitcast.83, bf16[512,2048]{1,0:T(8,128)(2,1)S(1)} %copy-done.3), kind=kOutput, calls=%fused_computation.146 | convolution fusion | flops 268435456 | bytes 3276800 | tf_op jit(solution)/shard_map/dot_general | solution.py:245
  129.0 2.9 %fusion.2 = bf16[128,2048]{1,0:T(8,128)(2,1)} fusion(f32[128,2048]{1,0:T(8,128)S(1)} %fusion.79, bf16[128,512]{0,1:T(8,128)(2,1)S(1)} %bitcast.82, bf16[512,2048]{1,0:T(8,128)(2,1)} %collective-permute-done.6, bf16[128,2048]{1,0:T(8,128)(2,1)S(1)} %copy-done.1, f32[2048]{0:T(1024)S(1)} %bitcast.86), kind=kOutput, calls=%fused_computation.3 | convolution fusion | flops 269746176 | bytes 4333568 | tf_op jit(solution)/shard_map/dot_general | solution.py:245
  (94 shorter events, 6.8 us)
Async XLA Ops:
  0.0 1.1 copy-start
  2.0 11.2 %copy-start.7 = (bf16[32,2048]{1,0:T(8,128)(2,1)S(1)}, bf16[32,2048]{1,0:T(8,128)(2,1)}, u32[]{:S(2)}) copy-start(bf16[32,2048]{1,0:T(8,128)(2,1)} %param.15) | copy-start | bytes 393220
  2.0 11.3 %copy-start.1 = (bf16[128,2048]{1,0:T(8,128)(2,1)S(1)}, bf16[128,2048]{1,0:T(8,128)(2,1)}, u32[]{:S(2)}) copy-start(bf16[128,2048]{1,0:T(8,128)(2,1)} %param.14) | copy-start | bytes 1572868
  3.6 15.3 %all-to-all-start = ((f32[32,1,896]{2,1,0:T(1,128)}), f32[32,1,896]{2,1,0:T(1,128)S(1)}, u32[]{:S(2)}, u32[]{:S(2)}) async-start(f32[32,1,896]{2,1,0:T(1,128)} %broadcast_in_dim.86), calls=%async_computation | async-start | bytes 229376 | tf_op jit(solution)/shard_map/all_to_all | solution.py:173
  10.9 16.4 %collective-permute-start.1 = (bf16[2048,256]{1,0:T(8,128)(2,1)}, bf16[2048,256]{1,0:T(8,128)(2,1)}, u32[]{:S(2)}, u32[]{:S(2)}) collective-permute-start(bf16[2048,256]{1,0:T(8,128)(2,1)} %param.20), channel_id=1, source_target_pairs={{0,1},{1,0},{2,3},{3,2},{4,5},{5,4},{6,7},{7,6},{8,9},{9,8},{10,11... | collective-permute-start | bytes 3145736 | tf_op jit(solution)/shard_map/ppermute | solution.py:28
  11.2 17.8 %collective-permute-start = (bf16[2048,256]{1,0:T(8,128)(2,1)}, bf16[2048,256]{1,0:T(8,128)(2,1)}, u32[]{:S(2)}, u32[]{:S(2)}) collective-permute-start(bf16[2048,256]{1,0:T(8,128)(2,1)} %param.19), channel_id=1, source_target_pairs={{0,1},{1,0},{2,3},{3,2},{4,5},{5,4},{6,7},{7,6},{8,9},{9,8},{10,11... | collective-permute-start | bytes 3145736 | tf_op jit(solution)/shard_map/ppermute | solution.py:28
  11.5 20.6 %collective-permute-start.4 = (bf16[2048,512]{1,0:T(8,128)(2,1)}, bf16[2048,512]{1,0:T(8,128)(2,1)}, u32[]{:S(2)}, u32[]{:S(2)}) collective-permute-start(bf16[2048,512]{1,0:T(8,128)(2,1)} %param.23), channel_id=1, source_target_pairs={{0,1},{1,0},{2,3},{3,2},{4,5},{5,4},{6,7},{7,6},{8,9},{9,8},{10,11... | collective-permute-start | bytes 6291464 | tf_op jit(solution)/shard_map/ppermute | solution.py:28
  11.8 11.5 %collective-permute-start.3 = (bf16[2048,256]{1,0:T(8,128)(2,1)}, bf16[2048,256]{1,0:T(8,128)(2,1)}, u32[]{:S(2)}, u32[]{:S(2)}) collective-permute-start(bf16[2048,256]{1,0:T(8,128)(2,1)} %param.22), channel_id=1, source_target_pairs={{0,1},{1,0},{2,3},{3,2},{4,5},{5,4},{6,7},{7,6},{8,9},{9,8},{10,11... | collective-permute-start | bytes 3145736 | tf_op jit(solution)/shard_map/ppermute | solution.py:28
  12.0 12.8 %collective-permute-start.2 = (bf16[2048,256]{1,0:T(8,128)(2,1)}, bf16[2048,256]{1,0:T(8,128)(2,1)}, u32[]{:S(2)}, u32[]{:S(2)}) collective-permute-start(bf16[2048,256]{1,0:T(8,128)(2,1)} %param.21), channel_id=1, source_target_pairs={{0,1},{1,0},{2,3},{3,2},{4,5},{5,4},{6,7},{7,6},{8,9},{9,8},{10,11... | collective-permute-start | bytes 3145736 | tf_op jit(solution)/shard_map/ppermute | solution.py:28
  19.3 0.6 copy-start.5
  19.5 9.5 %copy-start.8 = (bf16[16,2048]{1,0:T(8,128)(2,1)}, bf16[16,2048]{1,0:T(8,128)(2,1)S(1)}, u32[]{:S(2)}) copy-start(bf16[16,2048]{1,0:T(8,128)(2,1)S(1)} %fusion.40) | copy-start | bytes 196612
  19.9 2.1 %copy-start.11 = (bf16[2048,256]{1,0:T(8,128)(2,1)S(1)}, bf16[2048,256]{1,0:T(8,128)(2,1)}, u32[]{:S(2)}) copy-start(bf16[2048,256]{1,0:T(8,128)(2,1)} %param.21) | copy-start | bytes 3145732
  20.1 19.5 %copy-start.4 = (bf16[128,2048]{1,0:T(8,128)(2,1)}, bf16[128,2048]{1,0:T(8,128)(2,1)S(1)}, u32[]{:S(2)}) copy-start(bf16[128,2048]{1,0:T(8,128)(2,1)S(1)} %fusion.8) | copy-start | bytes 1572868
  20.1 2.2 %copy-start.10 = (bf16[2048,512]{1,0:T(8,128)(2,1)S(1)}, bf16[2048,512]{1,0:T(8,128)(2,1)}, u32[]{:S(2)}) copy-start(bf16[2048,512]{1,0:T(8,128)(2,1)} %param.23) | copy-start | bytes 6291460
  35.7 30.8 %all-to-all-start.2 = ((bf16[16,144,256]{2,1,0:T(8,128)(2,1)}), bf16[16,144,256]{2,1,0:T(8,128)(2,1)S(1)}, u32[]{:S(2)}, u32[]{:S(2)}) async-start(bf16[16,144,256]{2,1,0:T(8,128)(2,1)} %bitcast.72), calls=%async_computation.2 | async-start | bytes 2359296 | tf_op jit(solution)/shard_map/all_to_all | solution.py:230
  39.4 2.8 %copy-start.9 = (bf16[16,2048]{1,0:T(8,128)(2,1)S(1)}, bf16[16,2048]{1,0:T(8,128)(2,1)}, u32[]{:S(2)}) copy-start(bf16[16,2048]{1,0:T(8,128)(2,1)} %copy-done.8) | copy-start | bytes 196612
  39.4 2.8 %copy-start.12 = (bf16[2048,256]{1,0:T(8,128)(2,1)S(1)}, bf16[2048,256]{1,0:T(8,128)(2,1)}, u32[]{:S(2)}) copy-start(bf16[2048,256]{1,0:T(8,128)(2,1)} %param.20) | copy-start | bytes 3145732
  39.4 89.6 %collective-permute-start.6 = (bf16[512,2048]{1,0:T(8,128)(2,1)}, bf16[512,2048]{1,0:T(8,128)(2,1)}, u32[]{:S(2)}, u32[]{:S(2)}) collective-permute-start(bf16[512,2048]{1,0:T(8,128)(2,1)} %param.27), channel_id=1, source_target_pairs={{0,1},{1,0},{2,3},{3,2},{4,5},{5,4},{6,7},{7,6},{8,9},{9,8},{10,11... | collective-permute-start | bytes 6291464 | tf_op jit(solution)/shard_map/ppermute | solution.py:28
  66.5 30.7 %collective-permute-start.5 = (bf16[16,144,256]{2,1,0:T(8,128)(2,1)S(1)}, bf16[16,144,256]{2,1,0:T(8,128)(2,1)}, u32[]{:S(2)}, u32[]{:S(2)}) collective-permute-start(bf16[16,144,256]{2,1,0:T(8,128)(2,1)S(1)} %all-to-all-done.2), channel_id=1, source_target_pairs={{0,1},{1,0},{2,3},{3,2},{4,5},{5,4},{6,7},{7,6},{8,9},{9,8},{10,11... | collective-permute-start | bytes 3538952 | tf_op jit(solution)/shard_map/ppermute | solution.py:28
  66.7 3.8 %copy-start.6 = (bf16[144,256]{1,0:T(8,128)(2,1)S(1)}, bf16[144,256]{1,0:T(8,128)(2,1)}, u32[]{:S(2)}) copy-start(bf16[144,256]{1,0:T(8,128)(2,1)} %get-tuple-element.21) | copy-start | bytes 221188
  72.1 13.5 %all-to-all-start.1 = ((bf16[8,128,128]{2,1,0:T(8,128)(2,1)}), bf16[8,128,128]{2,1,0:T(8,128)(2,1)S(1)}, u32[]{:S(2)}, u32[]{:S(2)}) async-start(bf16[8,128,128]{2,1,0:T(8,128)(2,1)} %bitcast.15), calls=%async_computation.1 | async-start | bytes 524288 | tf_op jit(solution)/shard_map/all_to_all | solution.py:227
  85.6 0.7 copy-start.2
  101.1 26.5 %copy-start.3 = (bf16[512,2048]{1,0:T(8,128)(2,1)S(1)}, bf16[512,2048]{1,0:T(8,128)(2,1)}, u32[]{:S(2)}) copy-start(bf16[512,2048]{1,0:T(8,128)(2,1)} %param.27) | copy-start | bytes 6291460
  113.5 10.7 %all-to-all-start.3 = ((bf16[8,128,128]{2,1,0:T(8,128)(2,1)}), bf16[8,128,128]{2,1,0:T(8,128)(2,1)}, u32[]{:S(2)}, u32[]{:S(2)}) async-start(bf16[8,128,128]{2,1,0:T(8,128)(2,1)} %bitcast.78), calls=%async_computation.3 | async-start | bytes 524288 | tf_op jit(solution)/shard_map/all_to_all | solution.py:238

commit v2 on v1

v2 whole, which is shorter than its diff:
```python
import functools
import math

import jax
import jax.numpy as jnp
from jax import lax
from jax.experimental import pallas as pl
from jax.experimental.pallas import tpu as pltpu
from jax.sharding import Mesh, PartitionSpec as P

HEAD_DIM = 64
VALUE_DIM = 128
GRID_W = 64
EPSILON = 1e-06
THETA = 10000.0
SP = ("g", "s")
ALL = ("g", "s", "tp")


def norm_rows(rows):
    values = rows.astype(jnp.float32)
    return values * lax.rsqrt(jnp.mean(values * values, axis=-1, keepdims=True) + EPSILON)


def shifts_over(array, axis, size):
    out = [array]
    for k in range(1, size):
        out.append(lax.ppermute(array, axis, [(i, (i + k) % size) for i in range(size)]))
    return out


def rope_tables(positions, extra):
    quarter = HEAD_DIM // 4
    reciprocal = THETA ** (-jnp.arange(quarter, dtype=jnp.float32) / quarter)
    row = (positions // GRID_W).astype(jnp.float32)[:, None] * reciprocal[None, :]
    col = (positions % GRID_W).astype(jnp.float32)[:, None] * reciprocal[None, :]
    angle = jnp.concatenate([row, row, col, col] * 2, -1)
    sign = jnp.where((jnp.arange(2 * HEAD_DIM) // quarter) % 2 == 0, -1.0, 1.0)
    cosine = jnp.cos(angle)
    sine = jnp.sin(angle) * sign[None, :]
    width = angle.shape[1]
    cosine = jnp.concatenate([cosine, jnp.ones((extra, width), jnp.float32)], 0)
    sine = jnp.concatenate([sine, jnp.zeros((extra, width), jnp.float32)], 0)
    return cosine, sine


def projection_kernel(parts, kinds, heads_dev, copies, first_row, base, lat, ctx, mod, cos, sin, *refs):
    weights, outs = refs[: parts * kinds], refs[parts * kinds :]
    rows = lat.shape[0]
    h_lat = norm_rows(lat[...]) * (1.0 + mod[2:3, :]) + mod[0:1, :]
    h_ctx = norm_rows(ctx[...]) * (1.0 + mod[3:4, :]) + mod[1:2, :]
    h = jnp.concatenate([h_lat, h_ctx], 0).astype(jnp.bfloat16)
    cosine, sine = cos[...], sin[...]
    lane = lax.broadcasted_iota(jnp.int32, cosine.shape, 1)
    quarter = HEAD_DIM // 4
    lower = (lane // quarter) % 2 == 0
    heads = parts * heads_dev
    for k in range(parts):
        products = [
            jnp.dot(h, w[...], preferred_element_type=jnp.float32)
            for w in weights[k * kinds : (k + 1) * kinds]
        ]
        for j in range(heads_dev):
            pair = jnp.concatenate(
                [p[:, j * HEAD_DIM : (j + 1) * HEAD_DIM] for p in products[:2]], 1
            )
            flipped = jnp.where(
                lower,
                pltpu.roll(pair, 2 * HEAD_DIM - quarter, 1),
                pltpu.roll(pair, quarter, 1),
            )
            turned = (pair * cosine + flipped * sine).astype(jnp.bfloat16)
            if kinds == 3:
                value = products[2][:, j * VALUE_DIM : (j + 1) * VALUE_DIM]
                value = value.astype(jnp.bfloat16)
            for copy in range(copies):
                slot = copy * heads + base[k] + j
                begin = 0
                for n, out in enumerate(outs):
                    size = first_row[n + 1] - first_row[n]
                    pieces = [(0, size, first_row[n])]
                    if n == 0 and out.shape[1] > size:
                        pieces.append((size, out.shape[1] - size, rows))
                    for at, length, source in pieces:
                        out[slot, at : at + length, : 2 * HEAD_DIM] = turned[
                            source : source + length
                        ]
                        if kinds == 3:
                            out[slot, at : at + length, 2 * HEAD_DIM :] = value[
                                source : source + length
                            ]


def project(base, latent, context, mod, cosine, sine, weights, heads_dev, copies, bounds, extra):
    parts, kinds = len(weights), len(weights[0])
    width = 2 * HEAD_DIM + (VALUE_DIM if kinds == 3 else 0)
    shapes = [
        jax.ShapeDtypeStruct(
            (copies * parts * heads_dev, bounds[n + 1] - bounds[n] + (extra if n == 0 else 0), width),
            jnp.bfloat16,
        )
        for n in range(len(bounds) - 1)
    ]
    vmem = pl.BlockSpec(memory_space=pltpu.VMEM)
    flat = [w for part in weights for w in part]
    return pl.pallas_call(
        functools.partial(projection_kernel, parts, kinds, heads_dev, copies, bounds),
        in_specs=[pl.BlockSpec(memory_space=pltpu.SMEM)] + [vmem] * (5 + len(flat)),
        out_specs=[vmem] * len(shapes),
        out_shape=shapes,
        compiler_params=pltpu.CompilerParams(vmem_limit_bytes=56 * 2**20),
        name="project_kv" if kinds == 3 else "project_q",
    )(base, latent, context, mod, cosine, sine, *flat)


def attention_kernel(first, last, rows, parts, scal, gain, q_ref, *refs):
    refs = list(refs)
    kvs, refs = refs[:parts], refs[parts:]
    extra = kvs[0].shape[1] - rows
    scratch = 4 if extra else 2
    scratches, refs = refs[-scratch:], refs[:-scratch]
    if not first:
        old, refs = refs[:4], refs[4:]
    out = refs
    width = 2 * HEAD_DIM

    @pl.when(pl.program_id(0) == 0)
    def _():
        for n, (begin, length) in enumerate(((0, rows), (rows, extra))[: scratch // 2]):
            keys, vals = scratches[2 * n], scratches[2 * n + 1]
            place = 0
            for kv in kvs:
                for i in range(kv.shape[0]):
                    keys[place : place + length, :] = kv[i, begin : begin + length, :width]
                    vals[place : place + length, :VALUE_DIM] = kv[i, begin : begin + length, width:]
                    place += length
            vals[:, VALUE_DIM:] = jnp.ones((vals.shape[0], VALUE_DIM), vals.dtype)

    q = q_ref[...]
    lane = lax.broadcasted_iota(jnp.int32, q.shape, 1)
    dims = (((1,), (1,)), ((), ()))
    results = []
    for m in range(2):
        query = jnp.where((lane < HEAD_DIM) == (m == 0), q, jnp.zeros_like(q))
        scores = []
        for n in range(scratch // 2):
            s = lax.dot_general(
                query, scratches[2 * n][...], dims, preferred_element_type=jnp.float32
            )
            scores.append(s + scal[0] if n else s)
        peak = functools.reduce(jnp.maximum, [jnp.max(s, axis=-1, keepdims=True) for s in scores])
        if not first:
            before = old[2 + m][...][:, :1]
            peak = jnp.maximum(peak, before)
        acc = 0.0
        for n, s in enumerate(scores):
            p = jnp.exp2(s - peak).astype(jnp.bfloat16)
            acc = acc + jnp.dot(p, scratches[2 * n + 1][...], preferred_element_type=jnp.float32)
        if not first:
            acc = acc + old[m][...] * jnp.exp2(before - peak)
        if last:
            results.append(acc[:, :VALUE_DIM] / acc[:, VALUE_DIM:])
        else:
            out[m][...] = acc
            out[2 + m][...] = jnp.broadcast_to(peak, (q.shape[0], 128))
    if last:
        mixed = results[0] - scal[1] * results[1]
        scale = lax.rsqrt(jnp.mean(mixed * mixed, axis=-1, keepdims=True) + EPSILON)
        out[0][...] = (mixed * scale * gain[...]).astype(out[0].dtype)


def attend(scal, gain, queries, kvs, rows, state, last):
    count = queries.shape[0]
    tile = math.gcd(count, 256)
    rows_spec = lambda width: pl.BlockSpec((tile, width), lambda i: (i, 0))
    state_shapes = [jax.ShapeDtypeStruct((count, w), jnp.float32) for w in (256, 256, 128, 128)]
    state_specs = [rows_spec(s.shape[1]) for s in state_shapes]
    first = state is None
    if last:
        shapes = jax.ShapeDtypeStruct((count, VALUE_DIM), jnp.bfloat16)
        specs = rows_spec(VALUE_DIM)
    else:
        shapes, specs = state_shapes, state_specs
    sources = kvs[0].shape[0] * len(kvs)
    scratch = []
    for length in (rows, kvs[0].shape[1] - rows):
        if length:
            scratch.append(pltpu.VMEM((sources * length, 2 * HEAD_DIM), jnp.bfloat16))
            scratch.append(pltpu.VMEM((sources * length, 2 * VALUE_DIM), jnp.bfloat16))
    return pl.pallas_call(
        functools.partial(attention_kernel, first, last, rows, len(kvs)),
        grid=(count // tile,),
        in_specs=[
            pl.BlockSpec(memory_space=pltpu.SMEM),
            pl.BlockSpec(gain.shape, lambda i: (0, 0)),
            rows_spec(2 * HEAD_DIM),
        ]
        + [pl.BlockSpec(kv.shape, lambda i: (0, 0, 0)) for kv in kvs]
        + ([] if first else state_specs),
        out_specs=specs,
        out_shape=shapes,
        scratch_shapes=scratch,
        compiler_params=pltpu.CompilerParams(
            dimension_semantics=("arbitrary",), vmem_limit_bytes=56 * 2**20
        ),
        name="attend_last" if last else "attend_first" if first else "attend_next",
    )(scal, gain, queries, *kvs, *([] if first else state))


def body(
    latent,
    context,
    condition,
    context_condition,
    modulation_weight,
    query_first,
    query_second,
    key_first,
    key_second,
    value_weight,
    lambda_head,
    context_score_boost,
    head_gain,
    output_weight,
):
    width = latent.shape[1]
    tp = lax.axis_size("tp")
    sp = lax.axis_size(SP)
    groups = lax.axis_size("g")
    t = lax.axis_index("tp")
    head = lax.axis_index("s")
    heads_dev = value_weight.shape[1] // VALUE_DIM
    heads = heads_dev * tp

    signal = jax.nn.silu(jnp.stack([condition, context_condition])).astype(jnp.bfloat16)
    partial_mod = jnp.dot(signal, modulation_weight, preferred_element_type=jnp.float32)
    columns = partial_mod.shape[1]
    message = jnp.concatenate([partial_mod.reshape(-1), lambda_head, context_score_boost])
    pad = -message.shape[0] % 128
    message = jnp.pad(message, (0, pad))
    received = lax.all_to_all(
        jnp.broadcast_to(message[None], (sp * tp, message.shape[0])), ALL, 0, 0
    ).reshape(sp, tp, -1)
    modulation = jnp.sum(received[:, :, : 2 * columns], axis=1).reshape(sp, 2, columns)
    modulation = jnp.transpose(modulation, (1, 0, 2)).reshape(2, sp * columns)
    lambdas = received[0, :, 2 * columns : 2 * columns + heads_dev].reshape(heads)
    boosts = received[0, :, 2 * columns + heads_dev : 2 * columns + 2 * heads_dev].reshape(heads)
    scal = jnp.stack([boosts[head] * math.log2(math.e), lambdas[head]])
    shift = modulation[:, :width]
    scale = modulation[:, width : 2 * width]
    gate = modulation[0, 2 * width :]

    packs = [
        shifts_over(w, "tp", tp)
        for w in (query_first, query_second, key_first, key_second, value_weight)
    ]
    out_weights = shifts_over(output_weight, "tp", tp)
    rows = latent.shape[0]
    rows_ctx = context.shape[0] // tp
    ctx_own = lax.dynamic_slice_in_dim(context, t * rows_ctx, rows_ctx, 0)
    mod = jnp.concatenate([shift, scale], 0)
    offset = (lax.axis_index(SP) * tp + t) * rows
    cosine, sine = rope_tables(offset + jnp.arange(rows, dtype=jnp.int32), rows_ctx)
    base = ((t - jnp.arange(tp, dtype=jnp.int32)) % tp) * heads_dev

    factor = HEAD_DIM ** (-0.5) * math.log2(math.e)
    (q_all,) = project(
        base, latent, ctx_own, mod, cosine * factor, sine * factor,
        [[packs[0][k], packs[1][k]] for k in range(tp)], heads_dev, 1, (0, rows), 0,
    )
    queries = lax.all_to_all(q_all, "s", 0, 0).reshape(heads * rows, 2 * HEAD_DIM)
    half = rows // 2
    sent = project(
        base, latent, ctx_own, mod, cosine, sine,
        [[packs[n][k] for n in (2, 3, 4)] for k in range(tp)],
        heads_dev, groups, (0, half, rows), rows_ctx,
    )
    gain = head_gain[None, :]
    state, order = None, queries
    arrived = []
    for chunk in sent:
        chunk, order = lax.optimization_barrier((chunk, order))
        order = lax.all_to_all(chunk, SP, 0, 0)
        arrived.append(order)
    for n, kv in enumerate(arrived):
        state = attend(scal, gain, queries, shifts_over(kv, "tp", tp), half, state, n == 1)
    heads_out = lax.all_to_all(state.reshape(heads, rows, VALUE_DIM), "s", 0, 0)

    grouped = heads_out.reshape(tp, heads_dev, rows, VALUE_DIM)
    branch = 0.0
    for k in range(tp):
        own = lax.dynamic_index_in_dim(grouped, (t - k) % tp, 0, keepdims=False)
        own = jnp.transpose(own, (1, 0, 2)).reshape(rows, heads_dev * VALUE_DIM)
        branch = branch + jnp.dot(own, out_weights[k], preferred_element_type=jnp.float32)
    return (latent.astype(jnp.float32) + gate[None, :] * branch).astype(jnp.bfloat16)


def solution(mesh):
    sp, tp = mesh.shape["sp"], mesh.shape["tp"]

    def run(*args):
        heads = args[9].shape[1] // VALUE_DIM
        inner = Mesh(mesh.devices.reshape(sp // heads, heads, tp), ALL)
        in_specs = (
            P(ALL, None),
            P(SP, None),
            P("tp"),
            P("tp"),
            P("tp", SP),
            P(None, "tp"),
            P(None, "tp"),
            P(None, "tp"),
            P(None, "tp"),
            P(None, "tp"),
            P("tp"),
            P("tp"),
            P(),
            P("tp", None),
        )
        return jax.shard_map(
            body, mesh=inner, in_specs=in_specs, out_specs=P(ALL, None), check_vma=False
        )(*args)

    return run
```

time: 133 us -> 122 us (0.917)
  blocking collectives: 0 us -> 23.9 us
  local copies, waits for them, and re-layouts: 21.9 us -> 6.73 us
  matrix products: 19.1 us -> 5.82 us
  waiting for transfers between devices: 36 us -> 24.7 us
  Pallas kernels: 23.3 us -> 34.2 us
  starting transfers between devices: 22.8 us -> 19.6 us
  other arithmetic: 7.39 us -> 5.21 us
    all_to_all x0 -> x1, blocking collectives: none -> 23.9 us  [body(): order = lax.all_to_all(chunk, SP, 0, 0)]
    dot_general x10 -> x0, matrix products: 14 us -> none  [project(): product = jnp.dot(h, weight, preferred_element_type=jnp.float32)]
    pallas_call x2 -> x4, Pallas kernels: 23.3 us -> 34.2 us  [the longest x2 23.4 us: attend(): pl.pallas_call(functools.partial(attention_kernel, first, last, rows, len...]
    all_to_all x1, waiting for transfers between devices: 22.9 us -> 13.7 us  [body(): order = lax.all_to_all(chunk, SP, 0, 0)]
    slice x22 -> x2, local copies, waits for them, and re-layouts: 7.74 us -> 0.01 us  [the longest x1 0.01 us: body(): gate = modulation[0, 2 * width:]]
    convert_element_type x5 -> x0, other arithmetic: 3.26 us -> none  [the longest x3 2.94 us: project(): return product.astype(jnp.bfloat16).reshape(h.shape[0], heads_dev, -1)]
    reshape x14 -> x0, local copies, waits for them, and re-layouts: 2.89 us -> none  [project(): return product.astype(jnp.bfloat16).reshape(h.shape[0], heads_dev, -1)]
    all_to_all x1, starting transfers between devices: 6.18 us -> 3.41 us  [body(): lax.all_to_all(q_all, 's', 0, 0).reshape(heads * rows, 2 * HEAD_DIM)]
  transfers between devices with their start and end apart: 11 -> 12, of which waited for: 4 -> 3; matrix products, arithmetic and copies ran while one was open for 28% -> 8% of each run, Pallas kernels for 18% -> 28%
where the time goes in v2:
time: 122 us; the launch traced here: 121 us
  Pallas kernels  34.2 us (28%)
  waiting for transfers between devices  24.7 us (20%)
  blocking collectives  23.9 us (20%)
  starting transfers between devices  19.6 us (16%)
  local copies, waits for them, and re-layouts  6.73 us (6%)
  matrix products  5.82 us (5%)
  other arithmetic  5.21 us (4%)
    all_to_all x1, blocking collectives, body(): order = lax.all_to_all(chunk, SP, 0, 0)  23.9 us
    pallas_call x2, Pallas kernels, attend(): pl.pallas_call(functools.partial(attention_kernel, first, last, rows, len...  23.4 us
    all_to_all x1, waiting for transfers between devices, body(): order = lax.all_to_all(chunk, SP, 0, 0)  13.7 us
    pallas_call x2, Pallas kernels, project(): pl.pallas_call(functools.partial(projection_kernel, parts, kinds, heads_d...  10.8 us
    all_to_all x1, waiting for transfers between devices, body(): heads_out = lax.all_to_all(state.reshape(heads, rows, VALUE_DIM), 's', 0, 0)  7.44 us
    all_to_all x1, starting transfers between devices, body(): lax.all_to_all(jnp.broadcast_to(message[None], (sp * tp, message.shape[0]...  7.33 us
    dot_general x2, matrix products, body(): jnp.dot(own, out_weights[k], preferred_element_type=jnp.float32)  4.95 us
    unnamed x18, local copies, waits for them, and re-layouts  3.63 us
  transfers between devices with their start and end apart: 12, of which 3 were waited for; matrix products, arithmetic and copies ran while one was open for 8% of the time, Pallas kernels for 28%

profile of v2, /device:TPU:0, one launch (start us, length us, event | category | flops | bytes accessed | tf_op | source)
XLA Modules:
  0.0 121.1 jit_solution(10466946659929970832)
XLA Ops:
  0.0 1.1 copy-done
  1.1 0.9 fusion.4
  2.0 0.8 select_maximum_fusion
  2.8 0.7 broadcast_in_dim.10
  3.5 7.3 %all-to-all-start = ((f32[32,1,896]{2,1,0:T(1,128)}), f32[32,1,896]{2,1,0:T(1,128)S(1)}, u32[]{:S(2)}, u32[]{:S(2)}) async-start(f32[32,1,896]{2,1,0:T(1,128)} %broadcast_in_dim.10), calls=%async_computation | async-start | bytes 229376 | tf_op jit(solution)/shard_map/all_to_all | solution.py:241
  10.9 0.3 collective-permute-start
  11.2 0.3 collective-permute-start.1
  11.4 0.3 collective-permute-start.2
  11.7 0.3 collective-permute-start.3
  11.9 0.3 collective-permute-start.4
  12.2 0.1 broadcast_multiply_fusion.2
  12.3 0.2 concatenate.17
  12.5 0.2 sine_multiply_fusion
  12.8 0.7 fusion.15
  13.5 0.7 fusion.16
  14.1 0.5 fusion.7.base
  14.7 0.6 constant_dynamic-slice_fusion.2.ctx
  15.3 3.5 %all-to-all-done = f32[32,1,896]{2,1,0:T(1,128)S(1)} async-done(((f32[32,1,896]{2,1,0:T(1,128)}), f32[32,1,896]{2,1,0:T(1,128)S(1)}, u32[]{:S(2)}, u32[]{:S(2)}) %all-to-all-start) | async-done | bytes 114720 | tf_op jit(solution)/shard_map/all_to_all | solution.py:241
  18.8 0.3 reduce
  19.1 0.1 reshape.104
  19.2 0.1 slice_reduce_fusion
  19.3 0.6 pad_maximum_fusion.mod
  20.0 0.0 collective-permute-done.refs_2_
  20.0 4.3 %project_q.1 = bf16[8,128,128]{2,1,0:T(8,128)(2,1)} custom-call(s32[2]{0:T(128)} %fusion.7.base, bf16[128,2048]{1,0:T(8,128)(2,1)} %lat.3, bf16[16,2048]{1,0:T(8,128)(2,1)} %constant_dynamic-slice_fusion.2.ctx, f32[4,2048]{1,0:T(4,128)} %pad_maximum_fusion.mod, f32[144,128]{1,0:T(8,128)} %get-tuple-element.28.cos, f32[144,128]{1,0:T(8,128)} %get-tuple-element.26.sin, ...), custom_call_target="tpu_custom_call" | custom-call | tf_op jit(solution)/shard_map/project_q/pallas_call | solution.py:106
  24.3 3.4 %all-to-all-start.1 = ((bf16[8,128,128]{2,1,0:T(8,128)(2,1)}), bf16[8,128,128]{2,1,0:T(8,128)(2,1)S(1)}, u32[]{:S(2)}, u32[]{:S(2)}) async-start(bf16[8,128,128]{2,1,0:T(8,128)(2,1)} %project_q.1), calls=%async_computation.1 | async-start | bytes 524288 | tf_op jit(solution)/shard_map/all_to_all | solution.py:271
  27.7 0.0 collective-permute-done.2.refs_3_
  27.8 1.3 %copy-done.5 = bf16[2048,512]{1,0:T(8,128)(2,1)} copy-done((bf16[2048,512]{1,0:T(8,128)(2,1)}, bf16[2048,512]{1,0:T(8,128)(2,1)S(1)}, u32[]{:S(2)}) %copy-start.5) | copy-done | bytes 2097176
  29.1 6.5 %project_kv.1 = (bf16[16,80,256]{2,1,0:T(8,128)(2,1)}, bf16[16,64,256]{2,1,0:T(8,128)(2,1)}) custom-call(s32[2]{0:T(128)} %fusion.7.base, bf16[128,2048]{1,0:T(8,128)(2,1)} %lat.3, bf16[16,2048]{1,0:T(8,128)(2,1)} %constant_dynamic-slice_fusion.2.ctx, f32[4,2048]{1,0:T(4,128)} %pad_maximum_fusion.mod, f32[144,128]{1,0:T(8,128)} %get-tuple-element.27.cos, ...), custom_call_target="tpu_custom_call" | custom-call | tf_op jit(solution)/shard_map/project_kv/pallas_call | solution.py:106
  35.6 23.9 %all_to_all.26.refs_0_ = bf16[16,80,256]{2,1,0:T(8,128)(2,1)S(1)} all-to-all(bf16[16,80,256]{2,1,0:T(8,128)(2,1)} %get-tuple-element.15), channel_id=1, replica_groups=mesh['g'=2,'s'=8,'tp'=2] {'g','s'}, dimensions={0} | all-to-all | bytes 1310720 | tf_op jit(solution)/shard_map/all_to_all | solution.py:283
  59.5 3.6 %all-to-all-start.3 = ((bf16[16,64,256]{2,1,0:T(8,128)(2,1)}), bf16[16,64,256]{2,1,0:T(8,128)(2,1)S(1)}, u32[]{:S(2)}, u32[]{:S(2)}) async-start(bf16[16,64,256]{2,1,0:T(8,128)(2,1)} %get-tuple-element.16), calls=%async_computation.3 | async-start | bytes 1048576 | tf_op jit(solution)/shard_map/all_to_all | solution.py:283
  63.1 0.1 collective-permute-start.7
  63.2 0.5 collective-permute-start.6
  63.7 13.7 %all-to-all-done.3.refs_0_ = bf16[16,64,256]{2,1,0:T(8,128)(2,1)S(1)} async-done(((bf16[16,64,256]{2,1,0:T(8,128)(2,1)}), bf16[16,64,256]{2,1,0:T(8,128)(2,1)S(1)}, u32[]{:S(2)}, u32[]{:S(2)}) %all-to-all-start.3) | async-done | bytes 524320 | tf_op jit(solution)/shard_map/all_to_all | solution.py:283
  77.4 0.1 fusion.14
  77.4 0.1 reshape_squeeze.6
  77.5 0.1 reshape_squeeze.7
  77.6 0.6 dynamic_slice.16
  78.2 0.6 dynamic_slice.17
  79.4 1.2 pad_maximum_fusion.2.scal
  80.6 0.9 copy-done.6
  81.5 12.0 %attend_first.1 = (f32[1024,256]{1,0:T(8,128)}, f32[1024,256]{1,0:T(8,128)}, f32[1024,128]{1,0:T(8,128)}, f32[1024,128]{1,0:T(8,128)}) custom-call(f32[2]{0:T(128)} %pad_maximum_fusion.2.scal, f32[1,128]{1,0:T(1,128)} %bitcast.36, bf16[1024,128]{1,0:T(8,128)(2,1)} %bitcast.25, bf16[16,80,256]{2,1,0:T(8,128)(2,1)} %copy-done.2, bf16[16,80,256]{2,1,0:T(8,128)(2,1)} %copy-done.6), custom_call_target="tpu_custom_call" | custom-call | tf_op jit(solution)/shard_map/attend_first/pallas_call | solution.py:190
  93.4 11.5 %attend_last.1 = bf16[1024,128]{1,0:T(8,128)(2,1)} custom-call(f32[2]{0:T(128)} %pad_maximum_fusion.2.scal, f32[1,128]{1,0:T(1,128)} %bitcast.37, bf16[1024,128]{1,0:T(8,128)(2,1)} %bitcast.26, bf16[16,64,256]{2,1,0:T(8,128)(2,1)} %copy-done.4, bf16[16,64,256]{2,1,0:T(8,128)(2,1)} %collective-permute-done.5.refs_1_, f32[1024,256]{1,0:T(8,128)} %get-tuple-element.17.refs_2_, ...), custom_call_target="tpu_custom_call" | custom-call | tf_op jit(solution)/shard_map/attend_last/pallas_call | solution.py:190
  104.9 3.4 %all-to-all-start.4 = ((bf16[8,128,128]{2,1,0:T(8,128)(2,1)}), bf16[8,128,128]{2,1,0:T(8,128)(2,1)S(1)}, u32[]{:S(2)}, u32[]{:S(2)}) async-start(bf16[8,128,128]{2,1,0:T(8,128)(2,1)} %bitcast.27), calls=%async_computation.4 | async-start | bytes 524288 | tf_op jit(solution)/shard_map/all_to_all | solution.py:287
  108.4 7.4 %all-to-all-done.4 = bf16[8,128,128]{2,1,0:T(8,128)(2,1)S(1)} async-done(((bf16[8,128,128]{2,1,0:T(8,128)(2,1)}), bf16[8,128,128]{2,1,0:T(8,128)(2,1)S(1)}, u32[]{:S(2)}, u32[]{:S(2)}) %all-to-all-start.4) | async-done | bytes 262176 | tf_op jit(solution)/shard_map/all_to_all | solution.py:287
  115.8 0.1 copy.21
  116.0 0.1 copy.20
  116.1 2.1 %fusion.18 = f32[128,2048]{1,0:T(8,128)S(1)} fusion(bf16[128,512]{0,1:T(8,128)(2,1)S(1)} %bitcast.30, bf16[512,2048]{1,0:T(8,128)(2,1)} %param.27), kind=kOutput, calls=%fused_computation.52 | convolution fusion | flops 268435456 | bytes 3276800 | tf_op jit(solution)/shard_map/dot_general | solution.py:294
  118.2 2.9 %fusion.2 = bf16[128,2048]{1,0:T(8,128)(2,1)} fusion(f32[128,2048]{1,0:T(8,128)S(1)} %fusion.18, bf16[128,512]{0,1:T(8,128)(2,1)S(1)} %bitcast.29, bf16[512,2048]{1,0:T(8,128)(2,1)} %collective-permute-done.7, bf16[128,2048]{1,0:T(8,128)(2,1)S(1)} %copy-done.1, f32[2048]{0:T(1024)S(1)} %bitcast.33), kind=kOutput, calls=%fused_computation.3 | convolution fusion | flops 269746176 | bytes 4333568 | tf_op jit(solution)/shard_map/dot_general | solution.py:294
  (29 shorter events, 0.2 us)
Async XLA Ops:
  0.0 1.1 copy-start
  0.0 14.7 %copy-start.7 = (bf16[32,2048]{1,0:T(8,128)(2,1)S(1)}, bf16[32,2048]{1,0:T(8,128)(2,1)}, u32[]{:S(2)}) copy-start(bf16[32,2048]{1,0:T(8,128)(2,1)} %param.15) | copy-start | bytes 393220
  3.5 15.3 %all-to-all-start = ((f32[32,1,896]{2,1,0:T(1,128)}), f32[32,1,896]{2,1,0:T(1,128)S(1)}, u32[]{:S(2)}, u32[]{:S(2)}) async-start(f32[32,1,896]{2,1,0:T(1,128)} %broadcast_in_dim.10), calls=%async_computation | async-start | bytes 229376 | tf_op jit(solution)/shard_map/all_to_all | solution.py:241
  10.9 9.1 %collective-permute-start = (bf16[2048,256]{1,0:T(8,128)(2,1)}, bf16[2048,256]{1,0:T(8,128)(2,1)}, u32[]{:S(2)}, u32[]{:S(2)}) collective-permute-start(bf16[2048,256]{1,0:T(8,128)(2,1)} %refs_0_.2), channel_id=1, source_target_pairs={{0,1},{1,0},{2,3},{3,2},{4,5},{5,4},{6,7},{7,6},{8,9},{9,8},{10,11... | collective-permute-start | bytes 3145736 | tf_op jit(solution)/shard_map/ppermute | solution.py:28
  11.2 8.8 %collective-permute-start.1 = (bf16[2048,256]{1,0:T(8,128)(2,1)}, bf16[2048,256]{1,0:T(8,128)(2,1)}, u32[]{:S(2)}, u32[]{:S(2)}) collective-permute-start(bf16[2048,256]{1,0:T(8,128)(2,1)} %refs_1_.2), channel_id=1, source_target_pairs={{0,1},{1,0},{2,3},{3,2},{4,5},{5,4},{6,7},{7,6},{8,9},{9,8},{10,11... | collective-permute-start | bytes 3145736 | tf_op jit(solution)/shard_map/ppermute | solution.py:28
  11.4 16.3 %collective-permute-start.2 = (bf16[2048,256]{1,0:T(8,128)(2,1)}, bf16[2048,256]{1,0:T(8,128)(2,1)}, u32[]{:S(2)}, u32[]{:S(2)}) collective-permute-start(bf16[2048,256]{1,0:T(8,128)(2,1)} %refs_0_.3), channel_id=1, source_target_pairs={{0,1},{1,0},{2,3},{3,2},{4,5},{5,4},{6,7},{7,6},{8,9},{9,8},{10,11... | collective-permute-start | bytes 3145736 | tf_op jit(solution)/shard_map/ppermute | solution.py:28
  11.7 16.1 %collective-permute-start.3 = (bf16[2048,256]{1,0:T(8,128)(2,1)}, bf16[2048,256]{1,0:T(8,128)(2,1)}, u32[]{:S(2)}, u32[]{:S(2)}) collective-permute-start(bf16[2048,256]{1,0:T(8,128)(2,1)} %refs_1_.3), channel_id=1, source_target_pairs={{0,1},{1,0},{2,3},{3,2},{4,5},{5,4},{6,7},{7,6},{8,9},{9,8},{10,11... | collective-permute-start | bytes 3145736 | tf_op jit(solution)/shard_map/ppermute | solution.py:28
  11.9 15.8 %collective-permute-start.4 = (bf16[2048,512]{1,0:T(8,128)(2,1)}, bf16[2048,512]{1,0:T(8,128)(2,1)S(1)}, u32[]{:S(2)}, u32[]{:S(2)}) collective-permute-start(bf16[2048,512]{1,0:T(8,128)(2,1)} %refs_2_.1), channel_id=1, source_target_pairs={{0,1},{1,0},{2,3},{3,2},{4,5},{5,4},{6,7},{7,6},{8,9},{9,8},{10,11... | collective-permute-start | bytes 6291464 | tf_op jit(solution)/shard_map/ppermute | solution.py:28
  24.3 11.3 %all-to-all-start.1 = ((bf16[8,128,128]{2,1,0:T(8,128)(2,1)}), bf16[8,128,128]{2,1,0:T(8,128)(2,1)S(1)}, u32[]{:S(2)}, u32[]{:S(2)}) async-start(bf16[8,128,128]{2,1,0:T(8,128)(2,1)} %project_q.1), calls=%async_computation.1 | async-start | bytes 524288 | tf_op jit(solution)/shard_map/all_to_all | solution.py:271
  27.8 1.3 %copy-start.5 = (bf16[2048,512]{1,0:T(8,128)(2,1)}, bf16[2048,512]{1,0:T(8,128)(2,1)S(1)}, u32[]{:S(2)}) copy-start(bf16[2048,512]{1,0:T(8,128)(2,1)S(1)} %collective-permute-done.4.refs_5_) | copy-start | bytes 6291460
  35.6 45.0 %copy-start.3 = (bf16[8,128,128]{2,1,0:T(8,128)(2,1)}, bf16[8,128,128]{2,1,0:T(8,128)(2,1)S(1)}, u32[]{:S(2)}) copy-start(bf16[8,128,128]{2,1,0:T(8,128)(2,1)S(1)} %all-to-all-done.1) | copy-start | bytes 786436
  59.5 21.1 %copy-start.2 = (bf16[16,80,256]{2,1,0:T(8,128)(2,1)}, bf16[16,80,256]{2,1,0:T(8,128)(2,1)S(1)}, u32[]{:S(2)}) copy-start(bf16[16,80,256]{2,1,0:T(8,128)(2,1)S(1)} %all_to_all.26.refs_0_) | copy-start | bytes 1966084
  59.5 17.9 %all-to-all-start.3 = ((bf16[16,64,256]{2,1,0:T(8,128)(2,1)}), bf16[16,64,256]{2,1,0:T(8,128)(2,1)S(1)}, u32[]{:S(2)}, u32[]{:S(2)}) async-start(bf16[16,64,256]{2,1,0:T(8,128)(2,1)} %get-tuple-element.16), calls=%async_computation.3 | async-start | bytes 1048576 | tf_op jit(solution)/shard_map/all_to_all | solution.py:283
  63.1 55.1 %collective-permute-start.7 = (bf16[512,2048]{1,0:T(8,128)(2,1)}, bf16[512,2048]{1,0:T(8,128)(2,1)}, u32[]{:S(2)}, u32[]{:S(2)}) collective-permute-start(bf16[512,2048]{1,0:T(8,128)(2,1)} %param.27), channel_id=1, source_target_pairs={{0,1},{1,0},{2,3},{3,2},{4,5},{5,4},{6,7},{7,6},{8,9},{9,8},{10,11... | collective-permute-start | bytes 6291464 | tf_op jit(solution)/shard_map/ppermute | solution.py:28
  63.2 17.4 %collective-permute-start.6 = (bf16[16,80,256]{2,1,0:T(8,128)(2,1)S(1)}, bf16[16,80,256]{2,1,0:T(8,128)(2,1)S(1)}, u32[]{:S(2)}, u32[]{:S(2)}) collective-permute-start(bf16[16,80,256]{2,1,0:T(8,128)(2,1)S(1)} %all_to_all.26.refs_0_), channel_id=1, source_target_pairs={{0,1},{1,0},{2,3},{3,2},{4,5},{5,4},{6,7},{7,6},{8,9},{9,8},{10,11... | collective-permute-start | bytes 1966088 | tf_op jit(solution)/shard_map/ppermute | solution.py:28
  77.4 16.1 %copy-start.4 = (bf16[16,64,256]{2,1,0:T(8,128)(2,1)}, bf16[16,64,256]{2,1,0:T(8,128)(2,1)S(1)}, u32[]{:S(2)}) copy-start(bf16[16,64,256]{2,1,0:T(8,128)(2,1)S(1)} %all-to-all-done.3.refs_0_) | copy-start | bytes 1572868
  77.4 16.1 %collective-permute-start.5 = (bf16[16,64,256]{2,1,0:T(8,128)(2,1)S(1)}, bf16[16,64,256]{2,1,0:T(8,128)(2,1)}, u32[]{:S(2)}, u32[]{:S(2)}) collective-permute-start(bf16[16,64,256]{2,1,0:T(8,128)(2,1)S(1)} %all-to-all-done.3.refs_0_), channel_id=1, source_target_pairs={{0,1},{1,0},{2,3},{3,2},{4,5},{5,4},{6,7},{7,6},{8,9},{9,8},{10,11... | collective-permute-start | bytes 1572872 | tf_op jit(solution)/shard_map/ppermute | solution.py:28
  80.6 0.9 copy-start.6
  104.9 10.9 %all-to-all-start.4 = ((bf16[8,128,128]{2,1,0:T(8,128)(2,1)}), bf16[8,128,128]{2,1,0:T(8,128)(2,1)S(1)}, u32[]{:S(2)}, u32[]{:S(2)}) async-start(bf16[8,128,128]{2,1,0:T(8,128)(2,1)} %bitcast.27), calls=%async_computation.4 | async-start | bytes 524288 | tf_op jit(solution)/shard_map/all_to_all | solution.py:287
  115.8 2.4 %copy-start.1 = (bf16[128,2048]{1,0:T(8,128)(2,1)S(1)}, bf16[128,2048]{1,0:T(8,128)(2,1)}, u32[]{:S(2)}) copy-start(bf16[128,2048]{1,0:T(8,128)(2,1)} %lat.3) | copy-start | bytes 1572868

commit v3 on v2

--- a/solution.py
+++ b/solution.py
@@ -113,6 +113,13 @@
     )(base, latent, context, mod, cosine, sine, *flat)
 
 
+TILE = 512
+
+
+def weights_of(scores, peak):
+    return jnp.exp2(scores - peak).astype(jnp.bfloat16)
+
+
 def attention_kernel(first, last, rows, parts, scal, gain, q_ref, *refs):
     refs = list(refs)
     kvs, refs = refs[:parts], refs[parts:]
@@ -154,7 +161,7 @@
             peak = jnp.maximum(peak, before)
         acc = 0.0
         for n, s in enumerate(scores):
-            p = jnp.exp2(s - peak).astype(jnp.bfloat16)
+            p = weights_of(s, peak)
             acc = acc + jnp.dot(p, scratches[2 * n + 1][...], preferred_element_type=jnp.float32)
         if not first:
             acc = acc + old[m][...] * jnp.exp2(before - peak)
@@ -171,7 +178,7 @@
 
 def attend(scal, gain, queries, kvs, rows, state, last):
     count = queries.shape[0]
-    tile = math.gcd(count, 256)
+    tile = math.gcd(count, TILE)
     rows_spec = lambda width: pl.BlockSpec((tile, width), lambda i: (i, 0))
     state_shapes = [jax.ShapeDtypeStruct((count, w), jnp.float32) for w in (256, 256, 128, 128)]
     state_specs = [rows_spec(s.shape[1]) for s in state_shapes]
@@ -283,6 +290,8 @@
         order = lax.all_to_all(chunk, SP, 0, 0)
         arrived.append(order)
     for n, kv in enumerate(arrived):
+        if n:
+            kv, state = lax.optimization_barrier((kv, state))
         state = attend(scal, gain, queries, shifts_over(kv, "tp", tp), half, state, n == 1)
     heads_out = lax.all_to_all(state.reshape(heads, rows, VALUE_DIM), "s", 0, 0)
 

time: 122 us -> 112 us (0.918)
  waiting for transfers between devices: 24.7 us -> 13.6 us
  starting transfers between devices: 19.6 us -> 21.3 us
    all_to_all x1, waiting for transfers between devices: 13.7 us -> 0.01 us  [body(): order = lax.all_to_all(chunk, SP, 0, 0)]
    ppermute x8, waiting for transfers between devices: 0.02 us -> 3.24 us  [shifts_over(): lax.ppermute(array, axis, [(i, (i + k) % size) for i in range(size)])]
    all_to_all x1, starting transfers between devices: 3.41 us -> 4.74 us  [body(): heads_out = lax.all_to_all(state.reshape(heads, rows, VALUE_DIM), 's', 0, 0)]
    unnamed x18 -> x20, local copies, waits for them, and re-layouts: 3.63 us -> 4.43 us
  transfers between devices with their start and end apart: 12 -> 12, of which waited for: 3 -> 4; matrix products, arithmetic and copies ran while one was open for 8% -> 8% of each run, Pallas kernels for 28% -> 30%
where the time goes in v3:
time: 112 us
  Pallas kernels  33.2 us (30%)
  blocking collectives  23.9 us (21%)
  starting transfers between devices  21.3 us (19%)
  waiting for transfers between devices  13.6 us (12%)
  local copies, waits for them, and re-layouts  7.59 us (7%)
  matrix products  5.82 us (5%)
  other arithmetic  5.22 us (5%)
    all_to_all x1, blocking collectives, body(): order = lax.all_to_all(chunk, SP, 0, 0)  23.9 us
    pallas_call x2, Pallas kernels, attend(): pl.pallas_call(functools.partial(attention_kernel, first, last, rows, len...  22.4 us
    pallas_call x2, Pallas kernels, project(): pl.pallas_call(functools.partial(projection_kernel, parts, kinds, heads_d...  10.8 us
    all_to_all x1, starting transfers between devices, body(): lax.all_to_all(jnp.broadcast_to(message[None], (sp * tp, message.shape[0]...  7.33 us
    all_to_all x1, waiting for transfers between devices, body(): heads_out = lax.all_to_all(state.reshape(heads, rows, VALUE_DIM), 's', 0, 0)  6.9 us
    dot_general x2, matrix products, body(): jnp.dot(own, out_weights[k], preferred_element_type=jnp.float32)  4.95 us
    all_to_all x1, starting transfers between devices, body(): heads_out = lax.all_to_all(state.reshape(heads, rows, VALUE_DIM), 's', 0, 0)  4.74 us
    unnamed x20, local copies, waits for them, and re-layouts  4.43 us
  transfers between devices with their start and end apart: 12, of which 4 were waited for; matrix products, arithmetic and copies ran while one was open for 8% of the time, Pallas kernels for 30%

profile of v3, /device:TPU:0, one launch (start us, length us, event | category | flops | bytes accessed | tf_op | source)
XLA Modules:
  0.0 111.6 jit_solution(12547566380595645473)
XLA Ops:
  0.0 1.1 %copy-done = bf16[1024,384]{1,0:T(8,128)(2,1)S(1)} copy-done((bf16[1024,384]{1,0:T(8,128)(2,1)S(1)}, bf16[1024,384]{1,0:T(8,128)(2,1)}, u32[]{:S(2)}) %copy-start) | copy-done | bytes 786456
  1.1 0.9 fusion.4
  2.0 0.8 select_maximum_fusion
  2.8 0.7 broadcast_in_dim.10
  3.5 7.3 %all-to-all-start = ((f32[32,1,896]{2,1,0:T(1,128)}), f32[32,1,896]{2,1,0:T(1,128)S(1)}, u32[]{:S(2)}, u32[]{:S(2)}) async-start(f32[32,1,896]{2,1,0:T(1,128)} %broadcast_in_dim.10), calls=%async_computation | async-start | bytes 229376 | tf_op jit(solution)/shard_map/all_to_all | solution.py:248
  10.9 0.3 collective-permute-start
  11.2 0.3 collective-permute-start.1
  11.4 0.3 collective-permute-start.2
  11.7 0.3 collective-permute-start.3
  11.9 0.3 collective-permute-start.4
  12.2 0.1 broadcast_multiply_fusion.2
  12.3 0.2 concatenate.17
  12.5 0.2 sine_multiply_fusion
  12.8 0.7 fusion.15
  13.5 0.7 fusion.16
  14.1 0.6 fusion.7.base
  14.7 0.6 constant_dynamic-slice_fusion.2.ctx
  15.4 3.5 %all-to-all-done = f32[32,1,896]{2,1,0:T(1,128)S(1)} async-done(((f32[32,1,896]{2,1,0:T(1,128)}), f32[32,1,896]{2,1,0:T(1,128)S(1)}, u32[]{:S(2)}, u32[]{:S(2)}) %all-to-all-start) | async-done | bytes 114720 | tf_op jit(solution)/shard_map/all_to_all | solution.py:248
  18.8 0.3 reduce
  19.2 0.1 slice_reduce_fusion
  19.3 0.6 pad_maximum_fusion.mod
  20.0 4.3 %project_q.1 = bf16[8,128,128]{2,1,0:T(8,128)(2,1)} custom-call(s32[2]{0:T(128)} %fusion.7.base, bf16[128,2048]{1,0:T(8,128)(2,1)} %lat.3, bf16[16,2048]{1,0:T(8,128)(2,1)} %constant_dynamic-slice_fusion.2.ctx, f32[4,2048]{1,0:T(4,128)} %pad_maximum_fusion.mod, f32[144,128]{1,0:T(8,128)} %get-tuple-element.38.cos, f32[144,128]{1,0:T(8,128)} %get-tuple-element.36.sin, ...), custom_call_target="tpu_custom_call" | custom-call | tf_op jit(solution)/shard_map/project_q/pallas_call | solution.py:106
  24.3 3.4 %all-to-all-start.1 = ((bf16[8,128,128]{2,1,0:T(8,128)(2,1)}), bf16[8,128,128]{2,1,0:T(8,128)(2,1)S(1)}, u32[]{:S(2)}, u32[]{:S(2)}) async-start(bf16[8,128,128]{2,1,0:T(8,128)(2,1)} %project_q.1), calls=%async_computation.1 | async-start | bytes 524288 | tf_op jit(solution)/shard_map/all_to_all | solution.py:278
  27.8 1.3 %copy-done.5 = bf16[2048,512]{1,0:T(8,128)(2,1)} copy-done((bf16[2048,512]{1,0:T(8,128)(2,1)}, bf16[2048,512]{1,0:T(8,128)(2,1)S(1)}, u32[]{:S(2)}) %copy-start.5) | copy-done | bytes 2097176
  29.1 6.5 %project_kv.1 = (bf16[16,80,256]{2,1,0:T(8,128)(2,1)}, bf16[16,64,256]{2,1,0:T(8,128)(2,1)}) custom-call(s32[2]{0:T(128)} %fusion.7.base, bf16[128,2048]{1,0:T(8,128)(2,1)} %lat.3, bf16[16,2048]{1,0:T(8,128)(2,1)} %constant_dynamic-slice_fusion.2.ctx, f32[4,2048]{1,0:T(4,128)} %pad_maximum_fusion.mod, f32[144,128]{1,0:T(8,128)} %get-tuple-element.37.cos, ...), custom_call_target="tpu_custom_call" | custom-call | tf_op jit(solution)/shard_map/project_kv/pallas_call | solution.py:106
  35.6 23.9 %all_to_all.26.refs_0_ = bf16[16,80,256]{2,1,0:T(8,128)(2,1)S(1)} all-to-all(bf16[16,80,256]{2,1,0:T(8,128)(2,1)} %get-tuple-element.20), channel_id=1, replica_groups=mesh['g'=2,'s'=8,'tp'=2] {'g','s'}, dimensions={0} | all-to-all | bytes 1310720 | tf_op jit(solution)/shard_map/all_to_all | solution.py:290
  59.5 3.8 %all-to-all-start.3 = ((bf16[16,64,256]{2,1,0:T(8,128)(2,1)}), bf16[16,64,256]{2,1,0:T(8,128)(2,1)S(1)}, u32[]{:S(2)}, u32[]{:S(2)}) async-start(bf16[16,64,256]{2,1,0:T(8,128)(2,1)} %get-tuple-element.21), calls=%async_computation.3 | async-start | bytes 1048576 | tf_op jit(solution)/shard_map/all_to_all | solution.py:290
  63.2 0.1 collective-permute-start.7
  63.3 0.5 collective-permute-start.5
  63.8 0.1 fusion.14
  63.9 0.1 reshape_squeeze.6
  64.0 0.1 reshape_squeeze.7
  64.1 0.7 dynamic_slice.16
  64.7 0.6 dynamic_slice.17
  66.0 1.2 %pad_maximum_fusion.2.scal = f32[2]{0:T(128)} fusion(f32[1]{0:T(128)} %dynamic_slice.17, f32[1]{0:T(128)S(6)} %mul.76), kind=kLoop, calls=%fused_computation.42 | loop fusion | flops 2 | bytes 16 | tf_op jit(solution)/shard_map/stack | solution.py:255
  67.2 1.5 %collective-permute-done.5.refs_1_ = bf16[16,80,256]{2,1,0:T(8,128)(2,1)S(1)} collective-permute-done((bf16[16,80,256]{2,1,0:T(8,128)(2,1)S(1)}, bf16[16,80,256]{2,1,0:T(8,128)(2,1)S(1)}, u32[]{:S(2)}, u32[]{:S(2)}) %collective-permute-start.5) | collective-permute-done | bytes 655392 | tf_op jit(solution)/shard_map/ppermute | solution.py:28
  68.6 0.9 copy-done.6
  69.5 11.3 %attend_first.1 = (f32[1024,256]{1,0:T(8,128)}, f32[1024,256]{1,0:T(8,128)}, f32[1024,128]{1,0:T(8,128)}, f32[1024,128]{1,0:T(8,128)}) custom-call(f32[2]{0:T(128)} %pad_maximum_fusion.2.scal, f32[1,128]{1,0:T(1,128)} %bitcast.36, bf16[1024,128]{1,0:T(8,128)(2,1)} %bitcast.25, bf16[16,80,256]{2,1,0:T(8,128)(2,1)} %copy-done.2, bf16[16,80,256]{2,1,0:T(8,128)(2,1)} %copy-done.6), custom_call_target="tpu_custom_call" | custom-call | tf_op jit(solution)/shard_map/attend_first/pallas_call | solution.py:197
  80.9 0.2 collective-permute-start.6
  81.1 1.8 %collective-permute-done.6.refs_1_ = bf16[16,64,256]{2,1,0:T(8,128)(2,1)S(1)} collective-permute-done((bf16[16,64,256]{2,1,0:T(8,128)(2,1)S(1)}, bf16[16,64,256]{2,1,0:T(8,128)(2,1)S(1)}, u32[]{:S(2)}, u32[]{:S(2)}) %collective-permute-start.6) | collective-permute-done | bytes 524320 | tf_op jit(solution)/shard_map/ppermute | solution.py:28
  82.8 0.8 copy-done.7
  83.7 11.0 %attend_last.1 = bf16[1024,128]{1,0:T(8,128)(2,1)} custom-call(f32[2]{0:T(128)} %pad_maximum_fusion.2.scal, f32[1,128]{1,0:T(1,128)} %bitcast.37, bf16[1024,128]{1,0:T(8,128)(2,1)} %bitcast.26, bf16[16,64,256]{2,1,0:T(8,128)(2,1)} %copy-done.4, bf16[16,64,256]{2,1,0:T(8,128)(2,1)} %copy-done.7, f32[1024,256]{1,0:T(8,128)} %get-tuple-element.27.refs_2_, ...), custom_call_target="tpu_custom_call" | custom-call | tf_op jit(solution)/shard_map/attend_last/pallas_call | solution.py:197
  94.7 4.7 %all-to-all-start.4 = ((bf16[8,128,128]{2,1,0:T(8,128)(2,1)}), bf16[8,128,128]{2,1,0:T(8,128)(2,1)S(1)}, u32[]{:S(2)}, u32[]{:S(2)}) async-start(bf16[8,128,128]{2,1,0:T(8,128)(2,1)} %bitcast.27), calls=%async_computation.4 | async-start | bytes 524288 | tf_op jit(solution)/shard_map/all_to_all | solution.py:296
  99.4 6.9 %all-to-all-done.4 = bf16[8,128,128]{2,1,0:T(8,128)(2,1)S(1)} async-done(((bf16[8,128,128]{2,1,0:T(8,128)(2,1)}), bf16[8,128,128]{2,1,0:T(8,128)(2,1)S(1)}, u32[]{:S(2)}, u32[]{:S(2)}) %all-to-all-start.4) | async-done | bytes 262176 | tf_op jit(solution)/shard_map/all_to_all | solution.py:296
  106.4 0.1 copy.21
  106.5 0.1 copy.20
  106.6 2.1 %fusion.18 = f32[128,2048]{1,0:T(8,128)S(1)} fusion(bf16[128,512]{0,1:T(8,128)(2,1)S(1)} %bitcast.30, bf16[512,2048]{1,0:T(8,128)(2,1)} %param.27), kind=kOutput, calls=%fused_computation.52 | convolution fusion | flops 268435456 | bytes 3276800 | tf_op jit(solution)/shard_map/dot_general | solution.py:303
  108.7 2.9 %fusion.2 = bf16[128,2048]{1,0:T(8,128)(2,1)} fusion(f32[128,2048]{1,0:T(8,128)S(1)} %fusion.18, bf16[128,512]{0,1:T(8,128)(2,1)S(1)} %bitcast.29, bf16[512,2048]{1,0:T(8,128)(2,1)} %collective-permute-done.7, bf16[128,2048]{1,0:T(8,128)(2,1)S(1)} %copy-done.1, f32[2048]{0:T(1024)S(1)} %bitcast.33), kind=kOutput, calls=%fused_computation.3 | convolution fusion | flops 269746176 | bytes 4333568 | tf_op jit(solution)/shard_map/dot_general | solution.py:303
  (31 shorter events, 0.2 us)
Async XLA Ops:
  0.0 1.1 %copy-start = (bf16[1024,384]{1,0:T(8,128)(2,1)S(1)}, bf16[1024,384]{1,0:T(8,128)(2,1)}, u32[]{:S(2)}) copy-start(bf16[1024,384]{1,0:T(8,128)(2,1)} %param.18) | copy-start | bytes 2359300
  0.0 14.7 %copy-start.8 = (bf16[32,2048]{1,0:T(8,128)(2,1)S(1)}, bf16[32,2048]{1,0:T(8,128)(2,1)}, u32[]{:S(2)}) copy-start(bf16[32,2048]{1,0:T(8,128)(2,1)} %param.15) | copy-start | bytes 393220
  3.5 15.3 %all-to-all-start = ((f32[32,1,896]{2,1,0:T(1,128)}), f32[32,1,896]{2,1,0:T(1,128)S(1)}, u32[]{:S(2)}, u32[]{:S(2)}) async-start(f32[32,1,896]{2,1,0:T(1,128)} %broadcast_in_dim.10), calls=%async_computation | async-start | bytes 229376 | tf_op jit(solution)/shard_map/all_to_all | solution.py:248
  10.9 9.1 %collective-permute-start = (bf16[2048,256]{1,0:T(8,128)(2,1)}, bf16[2048,256]{1,0:T(8,128)(2,1)}, u32[]{:S(2)}, u32[]{:S(2)}) collective-permute-start(bf16[2048,256]{1,0:T(8,128)(2,1)} %refs_0_.2), channel_id=1, source_target_pairs={{0,1},{1,0},{2,3},{3,2},{4,5},{5,4},{6,7},{7,6},{8,9},{9,8},{10,11... | collective-permute-start | bytes 3145736 | tf_op jit(solution)/shard_map/ppermute | solution.py:28
  11.2 8.8 %collective-permute-start.1 = (bf16[2048,256]{1,0:T(8,128)(2,1)}, bf16[2048,256]{1,0:T(8,128)(2,1)}, u32[]{:S(2)}, u32[]{:S(2)}) collective-permute-start(bf16[2048,256]{1,0:T(8,128)(2,1)} %refs_1_.2), channel_id=1, source_target_pairs={{0,1},{1,0},{2,3},{3,2},{4,5},{5,4},{6,7},{7,6},{8,9},{9,8},{10,11... | collective-permute-start | bytes 3145736 | tf_op jit(solution)/shard_map/ppermute | solution.py:28
  11.4 16.3 %collective-permute-start.2 = (bf16[2048,256]{1,0:T(8,128)(2,1)}, bf16[2048,256]{1,0:T(8,128)(2,1)}, u32[]{:S(2)}, u32[]{:S(2)}) collective-permute-start(bf16[2048,256]{1,0:T(8,128)(2,1)} %refs_0_.3), channel_id=1, source_target_pairs={{0,1},{1,0},{2,3},{3,2},{4,5},{5,4},{6,7},{7,6},{8,9},{9,8},{10,11... | collective-permute-start | bytes 3145736 | tf_op jit(solution)/shard_map/ppermute | solution.py:28
  11.7 16.1 %collective-permute-start.3 = (bf16[2048,256]{1,0:T(8,128)(2,1)}, bf16[2048,256]{1,0:T(8,128)(2,1)}, u32[]{:S(2)}, u32[]{:S(2)}) collective-permute-start(bf16[2048,256]{1,0:T(8,128)(2,1)} %refs_1_.3), channel_id=1, source_target_pairs={{0,1},{1,0},{2,3},{3,2},{4,5},{5,4},{6,7},{7,6},{8,9},{9,8},{10,11... | collective-permute-start | bytes 3145736 | tf_op jit(solution)/shard_map/ppermute | solution.py:28
  11.9 15.8 %collective-permute-start.4 = (bf16[2048,512]{1,0:T(8,128)(2,1)}, bf16[2048,512]{1,0:T(8,128)(2,1)S(1)}, u32[]{:S(2)}, u32[]{:S(2)}) collective-permute-start(bf16[2048,512]{1,0:T(8,128)(2,1)} %refs_2_.1), channel_id=1, source_target_pairs={{0,1},{1,0},{2,3},{3,2},{4,5},{5,4},{6,7},{7,6},{8,9},{9,8},{10,11... | collective-permute-start | bytes 6291464 | tf_op jit(solution)/shard_map/ppermute | solution.py:28
  24.3 11.2 %all-to-all-start.1 = ((bf16[8,128,128]{2,1,0:T(8,128)(2,1)}), bf16[8,128,128]{2,1,0:T(8,128)(2,1)S(1)}, u32[]{:S(2)}, u32[]{:S(2)}) async-start(bf16[8,128,128]{2,1,0:T(8,128)(2,1)} %project_q.1), calls=%async_computation.1 | async-start | bytes 524288 | tf_op jit(solution)/shard_map/all_to_all | solution.py:278
  27.8 1.3 %copy-start.5 = (bf16[2048,512]{1,0:T(8,128)(2,1)}, bf16[2048,512]{1,0:T(8,128)(2,1)S(1)}, u32[]{:S(2)}) copy-start(bf16[2048,512]{1,0:T(8,128)(2,1)S(1)} %collective-permute-done.4.refs_5_) | copy-start | bytes 6291460
  35.6 33.1 %copy-start.3 = (bf16[8,128,128]{2,1,0:T(8,128)(2,1)}, bf16[8,128,128]{2,1,0:T(8,128)(2,1)S(1)}, u32[]{:S(2)}) copy-start(bf16[8,128,128]{2,1,0:T(8,128)(2,1)S(1)} %all-to-all-done.1) | copy-start | bytes 786436
  59.5 9.1 %copy-start.2 = (bf16[16,80,256]{2,1,0:T(8,128)(2,1)}, bf16[16,80,256]{2,1,0:T(8,128)(2,1)S(1)}, u32[]{:S(2)}) copy-start(bf16[16,80,256]{2,1,0:T(8,128)(2,1)S(1)} %all_to_all.26.refs_0_) | copy-start | bytes 1966084
  59.5 21.4 %all-to-all-start.3 = ((bf16[16,64,256]{2,1,0:T(8,128)(2,1)}), bf16[16,64,256]{2,1,0:T(8,128)(2,1)S(1)}, u32[]{:S(2)}, u32[]{:S(2)}) async-start(bf16[16,64,256]{2,1,0:T(8,128)(2,1)} %get-tuple-element.21), calls=%async_computation.3 | async-start | bytes 1048576 | tf_op jit(solution)/shard_map/all_to_all | solution.py:290
  63.2 45.5 %collective-permute-start.7 = (bf16[512,2048]{1,0:T(8,128)(2,1)}, bf16[512,2048]{1,0:T(8,128)(2,1)}, u32[]{:S(2)}, u32[]{:S(2)}) collective-permute-start(bf16[512,2048]{1,0:T(8,128)(2,1)} %param.27), channel_id=1, source_target_pairs={{0,1},{1,0},{2,3},{3,2},{4,5},{5,4},{6,7},{7,6},{8,9},{9,8},{10,11... | collective-permute-start | bytes 6291464 | tf_op jit(solution)/shard_map/ppermute | solution.py:28
  63.3 5.3 %collective-permute-start.5 = (bf16[16,80,256]{2,1,0:T(8,128)(2,1)S(1)}, bf16[16,80,256]{2,1,0:T(8,128)(2,1)S(1)}, u32[]{:S(2)}, u32[]{:S(2)}) collective-permute-start(bf16[16,80,256]{2,1,0:T(8,128)(2,1)S(1)} %all_to_all.26.refs_0_), channel_id=1, source_target_pairs={{0,1},{1,0},{2,3},{3,2},{4,5},{5,4},{6,7},{7,6},{8,9},{9,8},{10,11... | collective-permute-start | bytes 1966088 | tf_op jit(solution)/shard_map/ppermute | solution.py:28
  68.6 0.9 copy-start.6
  80.8 2.0 %copy-start.4 = (bf16[16,64,256]{2,1,0:T(8,128)(2,1)}, bf16[16,64,256]{2,1,0:T(8,128)(2,1)S(1)}, u32[]{:S(2)}) copy-start(bf16[16,64,256]{2,1,0:T(8,128)(2,1)S(1)} %all-to-all-done.3.refs_0_) | copy-start | bytes 1572868
  80.9 2.0 %collective-permute-start.6 = (bf16[16,64,256]{2,1,0:T(8,128)(2,1)S(1)}, bf16[16,64,256]{2,1,0:T(8,128)(2,1)S(1)}, u32[]{:S(2)}, u32[]{:S(2)}) collective-permute-start(bf16[16,64,256]{2,1,0:T(8,128)(2,1)S(1)} %all-to-all-done.3.refs_0_), channel_id=1, source_target_pairs={{0,1},{1,0},{2,3},{3,2},{4,5},{5,4},{6,7},{7,6},{8,9},{9,8},{10,11... | collective-permute-start | bytes 1572872 | tf_op jit(solution)/shard_map/ppermute | solution.py:28
  82.8 0.8 copy-start.7
  94.7 11.6 %all-to-all-start.4 = ((bf16[8,128,128]{2,1,0:T(8,128)(2,1)}), bf16[8,128,128]{2,1,0:T(8,128)(2,1)S(1)}, u32[]{:S(2)}, u32[]{:S(2)}) async-start(bf16[8,128,128]{2,1,0:T(8,128)(2,1)} %bitcast.27), calls=%async_computation.4 | async-start | bytes 524288 | tf_op jit(solution)/shard_map/all_to_all | solution.py:296
  106.3 2.4 %copy-start.1 = (bf16[128,2048]{1,0:T(8,128)(2,1)S(1)}, bf16[128,2048]{1,0:T(8,128)(2,1)}, u32[]{:S(2)}) copy-start(bf16[128,2048]{1,0:T(8,128)(2,1)} %lat.3) | copy-start | bytes 1572868
